TPU v7x, 256 devices: a whole 4x4x8 slice. The times are simulated.
256 devices in a mesh: sp: 64 (over z, x, core), tp: 4 (over y).
Axes of the slice: x: 4, y: 4, z: 8, core: 2. Of those that a mesh axis runs over, the one named last changes fastest.
Arguments:
- inputs: bfloat16 [32768, 2048], P('sp', 'tp'), may hold values from -45 to 45
- norm_gain: float32 [3, 2048], replicated, may hold values from 0.1 to 1.9
- w_value: bfloat16 [3, 2048, 1024], P(None, 'sp', 'tp'), may hold values from -0.125 to 0.125
- w_gate: bfloat16 [3, 2048, 1024], P(None, 'sp', 'tp'), may hold values from -0.125 to 0.125
- conv_taps: float32 [3, 31, 1024], P(None, None, 'tp'), may hold values from -5 to 5
- ln_gain: float32 [3, 1024], P(None, 'tp'), may hold values from 0.1 to 1.9
- ln_bias: float32 [3, 1024], P(None, 'tp'), may hold values from -3 to 3
- w_out: bfloat16 [3, 1024, 2048], P(None, 'tp', 'sp'), may hold values from -0.1875 to 0.1875
Outputs:
- stream: bfloat16 [32768, 2048], P('sp', 'tp')
All inputs are finite; a program needn't handle non-finite values.
Results may differ from a plain program's by a relative error of at most 0.01.
Values may be sent and summed in bfloat16 or wider, within the bound.
No kernel may reach another device: no remote copies, remote signals or barrier semaphores. Data moves between devices by JAX's collectives and lax.ppermute only.
A program may use at most 64 MiB of HBM per device.

v0:
```python
import functools

import jax
import jax.numpy as jnp
from jax import lax
from jax.experimental import pallas as pl
from jax.experimental.pallas import tpu as pltpu
from jax.sharding import Mesh, PartitionSpec as P


NZ, NX, NC, NY = 8, 4, 2, 4
HALO = 32
ROWS = 64
TILE = 8
DEPTH, WIDE = 32, 256
GROUP = NX * NC * DEPTH
SPAN = {"z": NZ, "x": NX, "y": NY}

PLANS = (
    dict(last="z", outer="y", inner="x"),
    dict(last="y", outer="x", inner="z"),
    dict(last="x", outer="y", inner="z"),
)


def swap_cores(v, core):
    lane = lax.broadcasted_iota(jnp.int32, v.shape, 1)
    other = jnp.where(
        lane % (2 * DEPTH) < DEPTH,
        pltpu.roll(v, GROUP - DEPTH, 1),
        pltpu.roll(v, DEPTH, 1),
    )
    return jnp.where(core == 1, other, v)


def to_relative(v, at_x, core):
    return swap_cores(pltpu.roll(v, (NX - at_x) * (NC * DEPTH), 1), core)


def to_absolute(v, at_x, core):
    return pltpu.roll(swap_cores(v, core), at_x * (NC * DEPTH), 1)


def prepare_kernel(info_ref, before_ref, x_ref, gain_ref, windows_ref, rel_ref, pad_ref):
    at_z, at_x, core = info_ref[1], info_ref[2], info_ref[3]
    lead = before_ref.shape[0]
    count, halves, window, group = windows_ref.shape
    rows = window - lead
    for half in range(halves):
        cols = slice(half * group, (half + 1) * group)
        pad_ref[:lead] = to_relative(before_ref[:, cols].astype(jnp.float32), at_x, core).astype(jnp.bfloat16)
        for k in range(count):
            turned = to_relative(x_ref[k * rows : (k + 1) * rows, cols].astype(jnp.float32), at_x, core)
            pad_ref[lead + k * rows : lead + (k + 1) * rows] = turned.astype(jnp.bfloat16)
        for k in range(count):
            windows_ref[k, half] = pad_ref[k * rows : k * rows + window]
    for layer in range(gain_ref.shape[0]):
        for d in range(NZ):
            row = gain_ref[layer, pl.ds((at_z + d) % NZ, 1), :]
            rel_ref[layer, d : d + 1, :] = to_relative(jnp.broadcast_to(row, (8, group)), at_x, core)[:1]


def prepare(info, before, x, gain):
    lead, width = before.shape
    rows = x.shape[0] // NY
    return pl.pallas_call(
        prepare_kernel,
        in_specs=[pl.BlockSpec(memory_space=pltpu.SMEM)] + [pl.BlockSpec(memory_space=pltpu.VMEM)] * 3,
        out_specs=[pl.BlockSpec(memory_space=pltpu.VMEM)] * 2,
        out_shape=[
            jax.ShapeDtypeStruct((NY, width // GROUP, rows + lead, GROUP), jnp.bfloat16),
            jax.ShapeDtypeStruct((gain.shape[0], NZ, GROUP), jnp.float32),
        ],
        scratch_shapes=[pltpu.VMEM((lead + x.shape[0], GROUP), jnp.bfloat16)],
        name="prepare",
    )(info, before, x, gain.reshape(-1, NZ, GROUP))


def one_module(layer, reach, info_ref, x_of, gain_ref, small_of, shard, waits, starts, store, hid_ref, glu_ref, fil_ref, norm_ref):
    rows_in = x_of(0).shape[0]
    rows = rows_in - HALO
    channels = NY * WIDE

    def matrix(kind, dy, zs):
        return jnp.concatenate(
            [shard(kind, dy, dz, dx, dc) for dz in zs for dx in range(NX) for dc in range(NC)], axis=0
        )

    total = jnp.zeros((rows_in, 1), jnp.float32)
    for dz in range(NZ):
        xf = x_of(dz).astype(jnp.float32)
        total = total + jnp.sum(xf * xf, axis=1, keepdims=True)
    scale = lax.rsqrt(total / (NZ * GROUP) + 1e-06)
    for dz in range(NZ):
        xf = x_of(dz).astype(jnp.float32)
        hid_ref[:rows_in, dz * GROUP : (dz + 1) * GROUP] = (xf * scale * gain_ref[layer, dz : dz + 1, :]).astype(
            jnp.bfloat16
        )

    lead = HALO - reach
    row = lax.broadcasted_iota(jnp.int32, (rows_in, 1), 0)
    ahead = row < info_ref[4 + layer]

    def block(dy, carry):
        for k in range(NY):

            @pl.when(dy == k)
            def _():
                for copy in waits[k]:
                    copy.wait()
                for copy in starts[k]:
                    copy.start()

        hidden = hid_ref[:rows_in]
        value = jnp.dot(hidden, matrix(0, dy, range(NZ)), preferred_element_type=jnp.float32)
        gate = jnp.dot(hidden, matrix(1, dy, range(NZ)), preferred_element_type=jnp.float32)
        glu = (value * jax.nn.sigmoid(gate)).astype(jnp.bfloat16).astype(jnp.float32)
        glu_ref[:rows_in] = jnp.where(ahead, 0.0, glu)
        for r in range(0, rows, ROWS):
            count = min(ROWS, rows - r)
            acc = jnp.zeros((count, WIDE), jnp.float32)
            for s in range(TILE):
                extra = TILE if s else 0
                part = jnp.zeros((count + extra, WIDE), jnp.float32)
                for tap in range(reach + 1):
                    if (tap + lead) % TILE == s:
                        at = r + tap + lead - s
                        part = part + small_of(dy, layer, tap) * glu_ref[at : at + count + extra, :]
                acc = acc + part[s : s + count]
            fil_ref[dy, r : r + count, :] = acc
        return carry

    lax.fori_loop(0, NY, block, 0)

    total = jnp.zeros((rows, 1), jnp.float32)
    square = jnp.zeros((rows, 1), jnp.float32)
    for dy in range(NY):
        f = fil_ref[dy, :rows]
        total = total + jnp.sum(f, axis=1, keepdims=True)
        square = square + jnp.sum(f * f, axis=1, keepdims=True)
    mean = total / channels
    scale = lax.rsqrt(square / channels - mean * mean + 1e-06)
    for dy in range(NY):
        v = (fil_ref[dy, :rows] - mean) * scale * small_of(dy, layer, reach + 1) + small_of(dy, layer, reach + 2)
        norm_ref[:rows, dy * WIDE : (dy + 1) * WIDE] = (v * jax.nn.sigmoid(v)).astype(jnp.bfloat16)

    def features(dz, carry):
        weight = jnp.concatenate([matrix(2, dy, (dz,)) for dy in range(NY)], axis=1)
        acc = lax.dot_general(
            norm_ref[:rows], weight, (((1,), (1,)), ((), ())), preferred_element_type=jnp.float32
        )
        store(dz, x_of(dz, HALO).astype(jnp.float32) + acc)
        return carry

    lax.fori_loop(0, NZ, features, 0)


def copies_of(plan, part_refs, held_ref, core, sems):
    n = SPAN[plan["last"]]
    half = held_ref.shape[2] // 2
    pairs = [[(part_refs[0], held_ref.at[0, 0]), (part_refs[1], held_ref.at[0, 1])]]
    for k in range(1, n // 2 + 1):
        mine, other = part_refs[2 * k : 2 * k + 2]
        here = jnp.where(core == 0, n - k, k)
        there = n - here
        if k < n // 2:
            to = lambda d, c: held_ref.at[d, c]
        else:
            here, there = core, 1 - core
            to = lambda d, c, k=k: held_ref.at[k, c, pl.ds(d * half, half)]
        pairs.append(
            [(part.at[c], to(d, c ^ swap)) for part, d, swap in ((mine, here, 0), (other, there, 1)) for c in range(NC)]
        )
    if plan["last"] != "y":
        pairs = [[pair for group in pairs for pair in group]]
    count = iter(range(sems.shape[0]))
    copies = [[pltpu.make_async_copy(*pair, sems.at[next(count)]) for pair in group] for group in pairs]
    return copies + [[]] * (NY - len(copies))


def modules_kernel(first, counts, reach, *refs):
    (info_ref, x_ref, gain_ref, small_ref), refs = refs[:4], refs[4:]
    part_refs = []
    for n in counts:
        part_refs.append(refs[:n])
        refs = refs[n:]
    out_ref, *refs = refs
    work, (mid_ref, *refs) = refs[:4], refs[4:]
    held_refs, sems = refs[: len(counts)], refs[len(counts) :]
    at_z, at_x, core, at_y = info_ref[1], info_ref[2], info_ref[3], info_ref[7]

    copies = [
        copies_of(PLANS[first + k], part_refs[k], held_refs[k], core, sems[k]) for k in range(len(counts))
    ]
    for group in copies[0][:2]:
        for copy in group:
            copy.start()
    starts = [[*groups[2:], [], []] for groups in copies]
    for k, groups in enumerate(copies[1:]):
        starts[k][2] = [copy for group in groups[:2] for copy in group]

    for k in range(len(counts)):
        layer = first + k
        plan, held_ref = PLANS[layer], held_refs[k]
        source = x_ref if k == 0 else mid_ref

        def x_of(dz, skip=0, source=source, layer=layer):
            return source[(at_z + dz) % NZ if layer == 0 else dz, skip:, :]

        def shard(kind, dy, dz, dx, dc, plan=plan, held_ref=held_ref):
            at = dict(x=dx, y=dy, z=dz)
            place = at[plan["last"]], dc, at[plan["outer"]], at[plan["inner"]]
            return held_ref[(*place, slice(kind * DEPTH, (kind + 1) * DEPTH))]

        def store(dz, new, layer=layer, k=k):
            if k < len(counts) - 1:
                mid_ref[dz] = new.astype(jnp.bfloat16)
            elif layer < len(PLANS) - 1:
                out_ref[dz] = new.astype(jnp.bfloat16)
            else:
                z = (at_z + dz) % NZ
                at = pl.multiple_of((z % 2) * GROUP, GROUP)
                out_ref[z // 2, :, pl.ds(at, GROUP)] = to_absolute(new, at_x, core).astype(jnp.bfloat16)

        one_module(
            layer, reach, info_ref, x_of, gain_ref,
            lambda dy, layer, i: small_ref[(at_y + dy) % NY, layer, i : i + 1, :],
            shard, copies[k], starts[k], store, *work,
        )


def modules(info, x, gain, small, parts, first):
    rows_in = x.shape[1]
    rows = rows_in - len(parts) * HALO
    vmem = pl.BlockSpec(memory_space=pltpu.VMEM)
    last = first + len(parts) == len(PLANS)
    plans = PLANS[first : first + len(parts)]
    return pl.pallas_call(
        functools.partial(modules_kernel, first, [len(p) for p in parts], small.shape[2] - 3),
        in_specs=[pl.BlockSpec(memory_space=pltpu.SMEM)]
        + [vmem] * 3
        + [pl.BlockSpec(memory_space=pl.ANY)] * sum(len(p) for p in parts),
        out_specs=vmem,
        out_shape=jax.ShapeDtypeStruct((NZ // 2, rows, 2 * GROUP) if last else (NZ, rows, GROUP), jnp.bfloat16),
        scratch_shapes=[
            pltpu.VMEM((rows_in, NZ * GROUP), jnp.bfloat16),
            pltpu.VMEM((rows_in, WIDE), jnp.float32),
            pltpu.VMEM((NY, rows_in - HALO, WIDE), jnp.float32),
            pltpu.VMEM((rows_in - HALO, NY * WIDE), jnp.bfloat16),
            pltpu.VMEM((NZ, rows_in - HALO, GROUP), jnp.bfloat16),
        ]
        + [
            pltpu.VMEM((SPAN[p["last"]], NC, SPAN[p["outer"]], SPAN[p["inner"]], 3 * DEPTH, WIDE), jnp.bfloat16)
            for p in plans
        ]
        + [
            pltpu.SemaphoreType.DMA((2 * len(p) - 2,)) for p in parts
        ],
        cost_estimate=pl.CostEstimate(
            flops=len(parts) * 6 * rows_in * 2048 * 1024,
            transcendentals=0,
            bytes_accessed=len(parts) * 6 * 2048 * 1024,
        ),
    )(info, x, gain, small, *[a for p in parts for a in p])


def shift(a, axis, by):
    n = SPAN[axis]
    return lax.ppermute(a, axis, [(i, (i + by) % n) for i in range(n)])


def to_each(a, axis):
    return lax.all_to_all(jnp.broadcast_to(a, (SPAN[axis], *a.shape)), axis, 0, 0, tiled=True)


def ring(block, axis):
    n = SPAN[axis]
    held = {0: block}
    up = down = block
    for k in range(1, n // 2):
        up, down = shift(up, axis, 1), shift(down, axis, -1)
        held[n - k], held[k] = up, down
    half = block.shape[0] // 2
    k = n // 2
    farthest = (shift(up[:half], axis, 1), shift(down[half:], axis, -1))
    return held, farthest


def gathered(block, axis):
    held, farthest = ring(block, axis)
    held[SPAN[axis] // 2] = jnp.concatenate(farthest)
    return jnp.stack([held[d] for d in range(SPAN[axis])])


def swapped(a):
    return lax.ppermute(a, "c", [(0, 1), (1, 0)])


def last_parts(block, axis, core):
    n = SPAN[axis]
    parts = [block, swapped(block)]
    moving = jnp.stack(parts)
    axes = ("c", "y") if axis == "y" else (axis, "c")
    at = lambda i, c: c * n + i if axis == "y" else i * NC + c
    route = [(at(i, c), at((i + 1 - 2 * c) % n, c)) for i in range(n) for c in range(NC)]
    for k in range(1, n // 2 + 1):
        if k == n // 2:
            half = block.shape[0] // 2
            moving = lax.dynamic_slice_in_dim(moving, core * half, half, 1)
        moving = lax.ppermute(moving, axes, route)
        parts += [moving, swapped(moving)]
    return parts


def shards(inputs, norm_gain, w_value, w_gate, conv_taps, ln_gain, ln_bias, w_out):
    layers = norm_gain.shape[0]
    rows = inputs.shape[0] // NY
    lead = layers * HALO
    at_z, at_x, core, at_y = (lax.axis_index(a) for a in ("z", "x", "c", "y"))
    at = ((at_z * NX + at_x) * NC + core) * NY + at_y
    firsts = [jnp.maximum((layers - k) * HALO - at * rows, 0) for k in range(layers)]
    info = jnp.stack([at, at_z, at_x, core, *firsts, at_y]).astype(jnp.int32)
    sp = NZ * NX * NC
    before = lax.ppermute(inputs[-lead:], ("z", "x", "c"), [(i, i + 1) for i in range(sp - 1)])
    windows, gain = prepare(info, before, inputs, norm_gain)
    x = lax.all_to_all(windows, "y", 0, 0, tiled=True).reshape(NZ, rows + lead, GROUP)
    own = jnp.concatenate((conv_taps, ln_gain[:, None], ln_bias[:, None]), axis=1)
    small = to_each(own, "y")
    packed = jnp.concatenate((w_value, w_gate, jnp.swapaxes(w_out, 1, 2)), axis=1)
    alone = packed[0]
    xs = jnp.stack([alone, shift(alone, "x", -1), shift(alone, "x", 2), shift(alone, "x", 1)])
    zs = to_each(packed[1:], "z")
    block0 = gathered(xs, "y")
    block0, zs = lax.optimization_barrier((block0, zs))
    zs = lax.dynamic_slice_in_dim(jnp.concatenate((zs, zs)), at_z, NZ)
    block1 = gathered(zs[:, 0], "x")
    block2 = gathered(zs[:, 1], "y")
    parts0 = last_parts(block0, "z", core)
    parts1 = last_parts(block1, "y", core)
    parts2 = last_parts(block2, "x", core)
    x = modules(info, x, gain, small, [parts0], 0)
    x = modules(info, x, gain, small, [parts1, parts2], 1)
    return lax.all_to_all(x, "y", 0, 0, tiled=True).reshape(inputs.shape)


def solution(mesh):
    mesh = Mesh(mesh.devices.reshape(NZ, NX, NC, NY), ("z", "x", "c", "y"))
    sp = ("z", "x", "c")
    in_specs = (
        P(sp, "y"),
        P(),
        P(None, sp, "y"),
        P(None, sp, "y"),
        P(None, None, "y"),
        P(None, "y"),
        P(None, "y"),
        P(None, "y", sp),
    )
    out_specs = P(sp, "y")
    return jax.shard_map(shards, mesh=mesh, in_specs=in_specs, out_specs=out_specs, check_vma=False)
```

profile of v0, /device:TPU:4, one launch (start us, length us, event | category | flops | bytes accessed | tf_op | source)
XLA Modules:
  0.0 229.0 jit_solution(17692810334684537873)
XLA Ops:
  0.0 0.8 pad_maximum_fusion.8
  0.8 1.0 broadcast_in_dim.15
  1.8 8.5 %all-to-all-start.2 = ((bf16[8,2,96,256]{3,2,1,0:T(8,128)(2,1)}), bf16[8,2,96,256]{3,2,1,0:T(8,128)(2,1)S(1)}, u32[]{:S(2)}, u32[]{:S(2)}) async-start(bf16[8,2,96,256]{3,2,1,0:T(8,128)(2,1)} %broadcast_in_dim.15), calls=%async_computation.2 | async-start | bytes 1572864 | tf_op jit(solution)/shard_map/all_to_all | solution.py:273
  10.3 1.3 collective-permute-start.3
  11.6 0.8 collective-permute-start.2
  12.4 1.1 collective-permute-start.1
  13.6 1.0 collective-permute-done.3
  14.5 2.7 %collective-permute-done.2 = bf16[96,256]{1,0:T(8,128)(2,1)S(1)} collective-permute-done((bf16[96,256]{1,0:T(8,128)(2,1)S(1)}, bf16[96,256]{1,0:T(8,128)(2,1)S(1)}, u32[]{:S(2)}, u32[]{:S(2)}) %collective-permute-start.2) | collective-permute-done | bytes 49184 | tf_op jit(solution)/shard_map/ppermute | solution.py:269
  17.3 3.1 %collective-permute-start.4 = (bf16[4,96,256]{2,1,0:T(8,128)(2,1)S(1)}, bf16[4,96,256]{2,1,0:T(8,128)(2,1)S(1)}, u32[]{:S(2)}, u32[]{:S(2)}) collective-permute-start(bf16[4,96,256]{2,1,0:T(8,128)(2,1)S(1)} %get-tuple-element.22), channel_id=1, source_target_pairs={{0,3},{1,0},{2,1},{3,2},{4,7},{5,4},{6,5},{7,6},{8,11},{9,8},{10,9... | collective-permute-start | bytes 589832 | tf_op jit(solution)/shard_map/ppermute | solution.py:269
  20.3 3.2 %collective-permute-done.4 = bf16[4,96,256]{2,1,0:T(8,128)(2,1)S(1)} collective-permute-done((bf16[4,96,256]{2,1,0:T(8,128)(2,1)S(1)}, bf16[4,96,256]{2,1,0:T(8,128)(2,1)S(1)}, u32[]{:S(2)}, u32[]{:S(2)}) %collective-permute-start.4) | collective-permute-done | bytes 196640 | tf_op jit(solution)/shard_map/ppermute | solution.py:269
  23.5 3.8 %collective-permute-start.7 = (bf16[2,96,256]{2,1,0:T(8,128)(2,1)S(1)}, bf16[2,96,256]{2,1,0:T(8,128)(2,1)S(1)}, u32[]{:S(2)}, u32[]{:S(2)}) collective-permute-start(bf16[2,96,256]{2,1,0:T(8,128)(2,1)S(1)} %slice.45), channel_id=1, source_target_pairs={{0,3},{1,0},{2,1},{3,2},{4,7},{5,4},{6,5},{7,6},{8,11},{9,8},{10,9... | collective-permute-start | bytes 294920 | tf_op jit(solution)/shard_map/ppermute | solution.py:269
  27.4 2.1 collective-permute-done.7
  29.5 3.7 %collective-permute-done.6 = bf16[2,96,256]{2,1,0:T(8,128)(2,1)S(1)} collective-permute-done((bf16[2,96,256]{2,1,0:T(8,128)(2,1)S(1)}, bf16[2,96,256]{2,1,0:T(8,128)(2,1)S(1)}, u32[]{:S(2)}, u32[]{:S(2)}) %collective-permute-start.6) | collective-permute-done | bytes 98336 | tf_op jit(solution)/shard_map/ppermute | solution.py:269
  33.4 0.3 fusion
  33.8 1.0 collective-permute-start.17
  34.8 1.7 collective-permute-start.18
  36.6 2.4 %collective-permute-start.26 = (bf16[8,96,256]{2,1,0:T(8,128)(2,1)S(1)}, bf16[8,96,256]{2,1,0:T(8,128)(2,1)S(1)}, u32[]{:S(2)}, u32[]{:S(2)}) collective-permute-start(bf16[8,96,256]{2,1,0:T(8,128)(2,1)S(1)} %get-tuple-element.19), channel_id=1, source_target_pairs={{0,3},{1,0},{2,1},{3,2},{4,7},{5,4},{6,5},{7,6},{8,11},{9,8},{10,9... | collective-permute-start | bytes 1179656 | tf_op jit(solution)/shard_map/ppermute | solution.py:269
  38.9 6.0 %collective-permute-done.17 = bf16[8,96,256]{2,1,0:T(8,128)(2,1)S(1)} collective-permute-done((bf16[8,96,256]{2,1,0:T(8,128)(2,1)S(1)}, bf16[8,96,256]{2,1,0:T(8,128)(2,1)S(1)}, u32[]{:S(2)}, u32[]{:S(2)}) %collective-permute-start.17) | collective-permute-done | bytes 393248 | tf_op jit(solution)/shard_map/ppermute | solution.py:269
  45.0 0.6 collective-permute-start.20
  45.6 2.0 collective-permute-start.19
  47.6 0.5 collective-permute-done.26
  48.1 3.6 %collective-permute-start.29 = (bf16[4,96,256]{2,1,0:T(8,128)(2,1)S(1)}, bf16[4,96,256]{2,1,0:T(8,128)(2,1)S(1)}, u32[]{:S(2)}, u32[]{:S(2)}) collective-permute-start(bf16[4,96,256]{2,1,0:T(8,128)(2,1)S(1)} %slice.51), channel_id=1, source_target_pairs={{0,3},{1,0},{2,1},{3,2},{4,7},{5,4},{6,5},{7,6},{8,11},{9,8},{10,9... | collective-permute-start | bytes 589832 | tf_op jit(solution)/shard_map/ppermute | solution.py:269
  51.8 0.3 collective-permute-start.28
  52.1 0.3 fusion.3
  52.5 0.1 pad_maximum_fusion.2
  52.7 0.8 copy-done.2
  53.5 0.3 copy-done.6
  53.8 0.6 collective-permute-start.9
  54.4 1.4 collective-permute-done.29
  55.8 3.7 %collective-permute-done.28 = bf16[4,96,256]{2,1,0:T(8,128)(2,1)S(1)} collective-permute-done((bf16[4,96,256]{2,1,0:T(8,128)(2,1)S(1)}, bf16[4,96,256]{2,1,0:T(8,128)(2,1)S(1)}, u32[]{:S(2)}, u32[]{:S(2)}) %collective-permute-start.28) | collective-permute-done | bytes 196640 | tf_op jit(solution)/shard_map/ppermute | solution.py:269
  59.5 0.3 fusion.2
  59.9 15.7 %collective-permute-done.9.refs_6_ = bf16[2,4,4,96,256]{4,3,2,1,0:T(8,128)(2,1)} collective-permute-done((bf16[2,4,4,96,256]{4,3,2,1,0:T(8,128)(2,1)S(1)}, bf16[2,4,4,96,256]{4,3,2,1,0:T(8,128)(2,1)}, u32[]{:S(2)}, u32[]{:S(2)}) %collective-permute-start.9) | collective-permute-done | bytes 1572896 | tf_op jit(solution)/shard_map/ppermute | solution.py:310
  75.6 2.1 pad_maximum_fusion
  77.7 1.2 collective-permute-start.22
  78.8 2.1 pad_maximum_fusion.1
  81.0 3.0 %collective-permute-start.31 = (bf16[2,4,8,96,256]{4,3,2,1,0:T(8,128)(2,1)}, bf16[2,4,8,96,256]{4,3,2,1,0:T(8,128)(2,1)}, u32[]{:S(2)}, u32[]{:S(2)}) collective-permute-start(bf16[2,4,8,96,256]{4,3,2,1,0:T(8,128)(2,1)} %pad_maximum_fusion.1), channel_id=1, source_target_pairs={{0,8},{4,28},{8,16},{12,4},{16,24},{20,12},{24,0},{28,20},{1,9},{5... | collective-permute-start | bytes 9437192 | tf_op jit(solution)/shard_map/ppermute | solution.py:310
  84.0 13.5 %collective-permute-done.11.refs_8_ = bf16[2,4,4,96,256]{4,3,2,1,0:T(8,128)(2,1)} collective-permute-done((bf16[2,4,4,96,256]{4,3,2,1,0:T(8,128)(2,1)}, bf16[2,4,4,96,256]{4,3,2,1,0:T(8,128)(2,1)}, u32[]{:S(2)}, u32[]{:S(2)}) %collective-permute-start.11) | collective-permute-done | bytes 1572896 | tf_op jit(solution)/shard_map/ppermute | solution.py:310
  97.5 0.5 collective-permute-start.12
  98.0 0.9 slice.33
  98.9 20.5 %collective-permute-done.13.refs_10_ = bf16[2,4,4,96,256]{4,3,2,1,0:T(8,128)(2,1)} collective-permute-done((bf16[2,4,4,96,256]{4,3,2,1,0:T(8,128)(2,1)}, bf16[2,4,4,96,256]{4,3,2,1,0:T(8,128)(2,1)}, u32[]{:S(2)}, u32[]{:S(2)}) %collective-permute-start.13) | collective-permute-done | bytes 1572896 | tf_op jit(solution)/shard_map/ppermute | solution.py:310
  119.4 1.9 collective-permute-start
  121.4 1.2 constant_dynamic-slice_fusion.2
  122.7 0.1 constant_dynamic-slice_fusion.1
  122.8 1.2 collective-permute-start.24
  124.1 1.5 constant_dynamic-slice_fusion
  125.6 3.0 %collective-permute-start.33 = (bf16[2,2,8,96,256]{4,3,2,1,0:T(8,128)(2,1)S(1)}, bf16[2,2,8,96,256]{4,3,2,1,0:T(8,128)(2,1)}, u32[]{:S(2)}, u32[]{:S(2)}) collective-permute-start(bf16[2,2,8,96,256]{4,3,2,1,0:T(8,128)(2,1)S(1)} %constant_dynamic-slice_fusion), channel_id=1, source_target_pairs={{0,8},{4,28},{8,16},{12,4},{16,24},{20,12},{24,0},{28,20},{1,9},{5... | collective-permute-start | bytes 4718600 | tf_op jit(solution)/shard_map/ppermute | solution.py:310
  128.6 1.4 collective-permute-start.23
  130.2 5.7 %collective-permute-done.15.refs_12_ = bf16[2,2,4,96,256]{4,3,2,1,0:T(8,128)(2,1)S(1)} collective-permute-done((bf16[2,2,4,96,256]{4,3,2,1,0:T(8,128)(2,1)S(1)}, bf16[2,2,4,96,256]{4,3,2,1,0:T(8,128)(2,1)S(1)}, u32[]{:S(2)}, u32[]{:S(2)}) %collective-permute-start.15) | collective-permute-done | bytes 786464 | tf_op jit(solution)/shard_map/ppermute | solution.py:310
  135.9 0.6 collective-permute-start.14
  136.4 8.2 %collective-permute-done.24.refs_8_ = bf16[2,2,8,96,256]{4,3,2,1,0:T(8,128)(2,1)} collective-permute-done((bf16[2,2,8,96,256]{4,3,2,1,0:T(8,128)(2,1)S(1)}, bf16[2,2,8,96,256]{4,3,2,1,0:T(8,128)(2,1)}, u32[]{:S(2)}, u32[]{:S(2)}) %collective-permute-start.24) | collective-permute-done | bytes 1572896 | tf_op jit(solution)/shard_map/ppermute | solution.py:310
  144.6 1.1 collective-permute-start.25
  145.7 0.9 collective-permute-done.33.refs_14_
  146.6 2.7 %collective-permute-start.34 = (bf16[2,2,8,96,256]{4,3,2,1,0:T(8,128)(2,1)}, bf16[2,2,8,96,256]{4,3,2,1,0:T(8,128)(2,1)}, u32[]{:S(2)}, u32[]{:S(2)}) collective-permute-start(bf16[2,2,8,96,256]{4,3,2,1,0:T(8,128)(2,1)} %collective-permute-done.33.refs_14_), channel_id=1, source_target_pairs={{0,4},{4,0},{1,5},{5,1},{2,6},{6,2},{3,7},{7,3},{8,12},{12,8},{9,1... | collective-permute-start | bytes 4718600 | tf_op jit(solution)/shard_map/ppermute | solution.py:296
  149.4 0.8 broadcast_in_dim.14
  150.2 4.1 %all-to-all-start.1 = ((f32[4,3,33,256]{3,2,1,0:T(8,128)}), f32[4,3,33,256]{3,2,1,0:T(8,128)}, u32[]{:S(2)}, u32[]{:S(2)}) async-start(f32[4,3,33,256]{3,2,1,0:T(8,128)} %broadcast_in_dim.14), calls=%async_computation.1 | async-start | bytes 983040 | tf_op jit(solution)/shard_map/all_to_all | solution.py:273
  154.5 0.6 copy.21
  155.1 0.7 stack.113.info_ref.refs_0_
  155.8 4.0 %prepare.1 = (bf16[4,2,224,256]{3,2,1,0:T(8,128)(2,1)}, f32[3,8,256]{2,1,0:T(8,128)}) custom-call(s32[8]{0:T(128)} %stack.113.info_ref.refs_0_, bf16[96,512]{1,0:T(8,128)(2,1)} %copy-done.12, bf16[512,512]{1,0:T(8,128)(2,1)} %x_ref.1, f32[3,8,256]{2,1,0:T(8,128)} %bitcast.74), custom_call_target="tpu_custom_call" | custom-call | tf_op jit(solution)/shard_map/prepare/pallas_call | solution.py:66
  159.8 4.2 %all-to-all-done.1.refs_3_ = f32[4,3,33,256]{3,2,1,0:T(8,128)} async-done(((f32[4,3,33,256]{3,2,1,0:T(8,128)}), f32[4,3,33,256]{3,2,1,0:T(8,128)}, u32[]{:S(2)}, u32[]{:S(2)}) %all-to-all-start.1) | async-done | bytes 405536 | tf_op jit(solution)/shard_map/all_to_all | solution.py:273
  164.0 17.6 %all_to_all.20 = bf16[4,2,224,256]{3,2,1,0:T(8,128)(2,1)} all-to-all(bf16[4,2,224,256]{3,2,1,0:T(8,128)(2,1)} %get-tuple-element.9), channel_id=1, replica_groups=mesh['z'=8,'x'=4,'c'=2,'y'=4] {'y'}, dimensions={0} | all-to-all | bytes 1835008 | tf_op jit(solution)/shard_map/all_to_all | solution.py:326
  181.6 14.9 %shard_map.82.refs_1_ = bf16[8,192,256]{2,1,0:T(8,128)(2,1)} custom-call(s32[8]{0:T(128)} %stack.113.info_ref.refs_0_, bf16[8,224,256]{2,1,0:T(8,128)(2,1)} %bitcast.60, f32[3,8,256]{2,1,0:T(8,128)} %get-tuple-element.10.refs_2_, f32[4,3,33,256]{3,2,1,0:T(8,128)} %all-to-all-done.1.refs_3_, bf16[4,4,96,256]{3,2,1,0:T(8,128)(2,1)} %copy-done, ...), custom_call_target="tpu_custom_call" | custom-call | flops 2818572288 | bytes 12582912 | tf_op jit(solution)/shard_map/pallas_call | solution.py:238
  196.5 20.1 %shard_map.83 = bf16[4,128,512]{2,1,0:T(8,128)(2,1)} custom-call(s32[8]{0:T(128)} %stack.113.info_ref.refs_0_, bf16[8,192,256]{2,1,0:T(8,128)(2,1)} %shard_map.82.refs_1_, f32[3,8,256]{2,1,0:T(8,128)} %get-tuple-element.10.refs_2_, f32[4,3,33,256]{3,2,1,0:T(8,128)} %all-to-all-done.1.refs_3_, bf16[4,8,96,256]{3,2,1,0:T(8,128)(2,1)} %copy-done.2, ...), custom_call_target="tpu_custom_call" | custom-call | flops 4831838208 | bytes 25165824 | tf_op jit(solution)/shard_map/pallas_call | solution.py:238
  216.7 11.5 %all_to_all.21 = bf16[4,128,512]{2,1,0:T(8,128)(2,1)S(1)} all-to-all(bf16[4,128,512]{2,1,0:T(8,128)(2,1)} %shard_map.83), channel_id=1, replica_groups=mesh['z'=8,'x'=4,'c'=2,'y'=4] {'y'}, dimensions={0} | all-to-all | bytes 1048576 | tf_op jit(solution)/shard_map/all_to_all | solution.py:343
  228.2 0.8 copy.23
  (79 shorter events, 1.2 us)
Async XLA Ops:
  0.0 10.3 %copy-start.8 = (bf16[3,256,32]{1,2,0:T(8,128)(2,1)S(1)}, bf16[3,256,32]{1,2,0:T(8,128)(2,1)}, u32[]{:S(2)}) copy-start(bf16[3,256,32]{1,2,0:T(8,128)(2,1)} %param.15) | copy-start | bytes 147460
  0.0 10.3 %copy-start.9 = (bf16[3,32,256]{2,1,0:T(8,128)(2,1)S(1)}, bf16[3,32,256]{2,1,0:T(8,128)(2,1)}, u32[]{:S(2)}) copy-start(bf16[3,32,256]{2,1,0:T(8,128)(2,1)} %param.11) | copy-start | bytes 147460
  0.0 10.3 %copy-start.10 = (bf16[3,32,256]{2,1,0:T(8,128)(2,1)S(1)}, bf16[3,32,256]{2,1,0:T(8,128)(2,1)}, u32[]{:S(2)}) copy-start(bf16[3,32,256]{2,1,0:T(8,128)(2,1)} %param.10) | copy-start | bytes 147460
  1.8 31.6 %all-to-all-start.2 = ((bf16[8,2,96,256]{3,2,1,0:T(8,128)(2,1)}), bf16[8,2,96,256]{3,2,1,0:T(8,128)(2,1)S(1)}, u32[]{:S(2)}, u32[]{:S(2)}) async-start(bf16[8,2,96,256]{3,2,1,0:T(8,128)(2,1)} %broadcast_in_dim.15), calls=%async_computation.2 | async-start | bytes 1572864 | tf_op jit(solution)/shard_map/all_to_all | solution.py:273
  10.3 4.2 %collective-permute-start.3 = (bf16[96,256]{1,0:T(8,128)(2,1)S(1)}, bf16[96,256]{1,0:T(8,128)(2,1)S(1)}, u32[]{:S(2)}, u32[]{:S(2)}) collective-permute-start(bf16[96,256]{1,0:T(8,128)(2,1)S(1)} %bitcast.69), channel_id=1, source_target_pairs={{0,8},{8,16},{16,24},{24,0},{1,9},{9,17},{17,25},{25,1},{2,10},{10... | collective-permute-start | bytes 147464 | tf_op jit(solution)/shard_map/ppermute | solution.py:269
  11.6 5.6 %collective-permute-start.2 = (bf16[96,256]{1,0:T(8,128)(2,1)S(1)}, bf16[96,256]{1,0:T(8,128)(2,1)S(1)}, u32[]{:S(2)}, u32[]{:S(2)}) collective-permute-start(bf16[96,256]{1,0:T(8,128)(2,1)S(1)} %bitcast.70), channel_id=1, source_target_pairs={{0,16},{8,24},{16,0},{24,8},{1,17},{9,25},{17,1},{25,9},{2,18},{10... | collective-permute-start | bytes 147464 | tf_op jit(solution)/shard_map/ppermute | solution.py:269
  12.4 4.8 %collective-permute-start.1 = (bf16[96,256]{1,0:T(8,128)(2,1)S(1)}, bf16[96,256]{1,0:T(8,128)(2,1)S(1)}, u32[]{:S(2)}, u32[]{:S(2)}) collective-permute-start(bf16[96,256]{1,0:T(8,128)(2,1)S(1)} %bitcast.71), channel_id=1, source_target_pairs={{0,24},{8,0},{16,8},{24,16},{1,25},{9,1},{17,9},{25,17},{2,26},{10... | collective-permute-start | bytes 147464 | tf_op jit(solution)/shard_map/ppermute | solution.py:269
  17.3 6.3 %collective-permute-start.4 = (bf16[4,96,256]{2,1,0:T(8,128)(2,1)S(1)}, bf16[4,96,256]{2,1,0:T(8,128)(2,1)S(1)}, u32[]{:S(2)}, u32[]{:S(2)}) collective-permute-start(bf16[4,96,256]{2,1,0:T(8,128)(2,1)S(1)} %get-tuple-element.22), channel_id=1, source_target_pairs={{0,3},{1,0},{2,1},{3,2},{4,7},{5,4},{6,5},{7,6},{8,11},{9,8},{10,9... | collective-permute-start | bytes 589832 | tf_op jit(solution)/shard_map/ppermute | solution.py:269
  20.3 7.0 %collective-permute-start.5 = (bf16[4,96,256]{2,1,0:T(8,128)(2,1)S(1)}, bf16[4,96,256]{2,1,0:T(8,128)(2,1)S(1)}, u32[]{:S(2)}, u32[]{:S(2)}) collective-permute-start(bf16[4,96,256]{2,1,0:T(8,128)(2,1)S(1)} %get-tuple-element.22), channel_id=1, source_target_pairs={{0,1},{1,2},{2,3},{3,0},{4,5},{5,6},{6,7},{7,4},{8,9},{9,10},{10,1... | collective-permute-start | bytes 589832 | tf_op jit(solution)/shard_map/ppermute | solution.py:269
  23.5 6.0 %collective-permute-start.7 = (bf16[2,96,256]{2,1,0:T(8,128)(2,1)S(1)}, bf16[2,96,256]{2,1,0:T(8,128)(2,1)S(1)}, u32[]{:S(2)}, u32[]{:S(2)}) collective-permute-start(bf16[2,96,256]{2,1,0:T(8,128)(2,1)S(1)} %slice.45), channel_id=1, source_target_pairs={{0,3},{1,0},{2,1},{3,2},{4,7},{5,4},{6,5},{7,6},{8,11},{9,8},{10,9... | collective-permute-start | bytes 294920 | tf_op jit(solution)/shard_map/ppermute | solution.py:269
  27.3 5.9 %collective-permute-start.6 = (bf16[2,96,256]{2,1,0:T(8,128)(2,1)S(1)}, bf16[2,96,256]{2,1,0:T(8,128)(2,1)S(1)}, u32[]{:S(2)}, u32[]{:S(2)}) collective-permute-start(bf16[2,96,256]{2,1,0:T(8,128)(2,1)S(1)} %slice.44), channel_id=1, source_target_pairs={{0,1},{1,2},{2,3},{3,0},{4,5},{5,6},{6,7},{7,4},{8,9},{9,10},{10,1... | collective-permute-start | bytes 294920 | tf_op jit(solution)/shard_map/ppermute | solution.py:269
  33.4 19.2 %copy-start = (bf16[4,4,96,256]{3,2,1,0:T(8,128)(2,1)}, bf16[4,4,96,256]{3,2,1,0:T(8,128)(2,1)S(1)}, u32[]{:S(2)}) copy-start(bf16[4,4,96,256]{3,2,1,0:T(8,128)(2,1)S(1)} %pad_maximum_fusion.5.refs_4_) | copy-start | bytes 2359300
  33.8 11.1 %collective-permute-start.17 = (bf16[8,96,256]{2,1,0:T(8,128)(2,1)S(1)}, bf16[8,96,256]{2,1,0:T(8,128)(2,1)S(1)}, u32[]{:S(2)}, u32[]{:S(2)}) collective-permute-start(bf16[8,96,256]{2,1,0:T(8,128)(2,1)S(1)} %get-tuple-element.20), channel_id=1, source_target_pairs={{0,24},{8,0},{16,8},{24,16},{1,25},{9,1},{17,9},{25,17},{2,26},{10... | collective-permute-start | bytes 1179656 | tf_op jit(solution)/shard_map/ppermute | solution.py:269
  34.8 10.7 %collective-permute-start.18 = (bf16[8,96,256]{2,1,0:T(8,128)(2,1)S(1)}, bf16[8,96,256]{2,1,0:T(8,128)(2,1)S(1)}, u32[]{:S(2)}, u32[]{:S(2)}) collective-permute-start(bf16[8,96,256]{2,1,0:T(8,128)(2,1)S(1)} %get-tuple-element.20), channel_id=1, source_target_pairs={{0,8},{8,16},{16,24},{24,0},{1,9},{9,17},{17,25},{25,1},{2,10},{10... | collective-permute-start | bytes 1179656 | tf_op jit(solution)/shard_map/ppermute | solution.py:269
  36.6 15.9 %collective-permute-start.8 = (bf16[4,4,96,256]{3,2,1,0:T(8,128)(2,1)S(1)}, bf16[4,4,96,256]{3,2,1,0:T(8,128)(2,1)S(1)}, u32[]{:S(2)}, u32[]{:S(2)}) collective-permute-start(bf16[4,4,96,256]{3,2,1,0:T(8,128)(2,1)S(1)} %pad_maximum_fusion.5.refs_4_), channel_id=1, source_target_pairs={{0,4},{4,0},{1,5},{5,1},{2,6},{6,2},{3,7},{7,3},{8,12},{12,8},{9,1... | collective-permute-start | bytes 2359304 | tf_op jit(solution)/shard_map/ppermute | solution.py:296
  36.6 11.5 %collective-permute-start.26 = (bf16[8,96,256]{2,1,0:T(8,128)(2,1)S(1)}, bf16[8,96,256]{2,1,0:T(8,128)(2,1)S(1)}, u32[]{:S(2)}, u32[]{:S(2)}) collective-permute-start(bf16[8,96,256]{2,1,0:T(8,128)(2,1)S(1)} %get-tuple-element.19), channel_id=1, source_target_pairs={{0,3},{1,0},{2,1},{3,2},{4,7},{5,4},{6,5},{7,6},{8,11},{9,8},{10,9... | collective-permute-start | bytes 1179656 | tf_op jit(solution)/shard_map/ppermute | solution.py:269
  38.9 12.8 %collective-permute-start.27 = (bf16[8,96,256]{2,1,0:T(8,128)(2,1)S(1)}, bf16[8,96,256]{2,1,0:T(8,128)(2,1)S(1)}, u32[]{:S(2)}, u32[]{:S(2)}) collective-permute-start(bf16[8,96,256]{2,1,0:T(8,128)(2,1)S(1)} %get-tuple-element.19), channel_id=1, source_target_pairs={{0,1},{1,2},{2,3},{3,0},{4,5},{5,6},{6,7},{7,4},{8,9},{9,10},{10,1... | collective-permute-start | bytes 1179656 | tf_op jit(solution)/shard_map/ppermute | solution.py:269
  45.0 7.1 %collective-permute-start.20 = (bf16[4,96,256]{2,1,0:T(8,128)(2,1)S(1)}, bf16[4,96,256]{2,1,0:T(8,128)(2,1)S(1)}, u32[]{:S(2)}, u32[]{:S(2)}) collective-permute-start(bf16[4,96,256]{2,1,0:T(8,128)(2,1)S(1)} %slice.48), channel_id=1, source_target_pairs={{0,24},{8,0},{16,8},{24,16},{1,25},{9,1},{17,9},{25,17},{2,26},{10... | collective-permute-start | bytes 589832 | tf_op jit(solution)/shard_map/ppermute | solution.py:269
  45.6 6.5 %collective-permute-start.19 = (bf16[4,96,256]{2,1,0:T(8,128)(2,1)S(1)}, bf16[4,96,256]{2,1,0:T(8,128)(2,1)S(1)}, u32[]{:S(2)}, u32[]{:S(2)}) collective-permute-start(bf16[4,96,256]{2,1,0:T(8,128)(2,1)S(1)} %slice.47), channel_id=1, source_target_pairs={{0,8},{8,16},{16,24},{24,0},{1,9},{9,17},{17,25},{25,1},{2,10},{10... | collective-permute-start | bytes 589832 | tf_op jit(solution)/shard_map/ppermute | solution.py:269
  48.1 7.6 %collective-permute-start.29 = (bf16[4,96,256]{2,1,0:T(8,128)(2,1)S(1)}, bf16[4,96,256]{2,1,0:T(8,128)(2,1)S(1)}, u32[]{:S(2)}, u32[]{:S(2)}) collective-permute-start(bf16[4,96,256]{2,1,0:T(8,128)(2,1)S(1)} %slice.51), channel_id=1, source_target_pairs={{0,3},{1,0},{2,1},{3,2},{4,7},{5,4},{6,5},{7,6},{8,11},{9,8},{10,9... | collective-permute-start | bytes 589832 | tf_op jit(solution)/shard_map/ppermute | solution.py:269
  51.8 7.6 %collective-permute-start.28 = (bf16[4,96,256]{2,1,0:T(8,128)(2,1)S(1)}, bf16[4,96,256]{2,1,0:T(8,128)(2,1)S(1)}, u32[]{:S(2)}, u32[]{:S(2)}) collective-permute-start(bf16[4,96,256]{2,1,0:T(8,128)(2,1)S(1)} %slice.50), channel_id=1, source_target_pairs={{0,1},{1,2},{2,3},{3,0},{4,5},{5,6},{6,7},{7,4},{8,9},{9,10},{10,1... | collective-permute-start | bytes 589832 | tf_op jit(solution)/shard_map/ppermute | solution.py:269
  52.4 1.1 copy-start.2
  52.4 23.2 %collective-permute-start.21 = (bf16[4,8,96,256]{3,2,1,0:T(8,128)(2,1)S(1)}, bf16[4,8,96,256]{3,2,1,0:T(8,128)(2,1)S(1)}, u32[]{:S(2)}, u32[]{:S(2)}) collective-permute-start(bf16[4,8,96,256]{3,2,1,0:T(8,128)(2,1)S(1)} %get-tuple-element.16.refs_4_), channel_id=1, source_target_pairs={{0,4},{4,0},{1,5},{5,1},{2,6},{6,2},{3,7},{7,3},{8,12},{12,8},{9,1... | collective-permute-start | bytes 4718600 | tf_op jit(solution)/shard_map/ppermute | solution.py:296
  52.5 1.3 copy-start.6
  53.8 21.7 %collective-permute-start.9 = (bf16[2,4,4,96,256]{4,3,2,1,0:T(8,128)(2,1)S(1)}, bf16[2,4,4,96,256]{4,3,2,1,0:T(8,128)(2,1)}, u32[]{:S(2)}, u32[]{:S(2)}) collective-permute-start(bf16[2,4,4,96,256]{4,3,2,1,0:T(8,128)(2,1)S(1)} %pad_maximum_fusion.2), channel_id=1, source_target_pairs={{0,32},{4,228},{32,64},{36,4},{64,96},{68,36},{96,128},{100,68},{1... | collective-permute-start | bytes 4718600 | tf_op jit(solution)/shard_map/ppermute | solution.py:310
  59.7 17.9 %copy-start.4 = (bf16[4,8,96,256]{3,2,1,0:T(8,128)(2,1)}, bf16[4,8,96,256]{3,2,1,0:T(8,128)(2,1)S(1)}, u32[]{:S(2)}) copy-start(bf16[4,8,96,256]{3,2,1,0:T(8,128)(2,1)S(1)} %get-tuple-element.14.refs_10_) | copy-start | bytes 4718596
  59.8 19.1 %collective-permute-start.30 = (bf16[4,8,96,256]{3,2,1,0:T(8,128)(2,1)S(1)}, bf16[4,8,96,256]{3,2,1,0:T(8,128)(2,1)S(1)}, u32[]{:S(2)}, u32[]{:S(2)}) collective-permute-start(bf16[4,8,96,256]{3,2,1,0:T(8,128)(2,1)S(1)} %get-tuple-element.14.refs_10_), channel_id=1, source_target_pairs={{0,4},{4,0},{1,5},{5,1},{2,6},{6,2},{3,7},{7,3},{8,12},{12,8},{9,1... | collective-permute-start | bytes 4718600 | tf_op jit(solution)/shard_map/ppermute | solution.py:296
  75.6 21.9 %collective-permute-start.11 = (bf16[2,4,4,96,256]{4,3,2,1,0:T(8,128)(2,1)}, bf16[2,4,4,96,256]{4,3,2,1,0:T(8,128)(2,1)}, u32[]{:S(2)}, u32[]{:S(2)}) collective-permute-start(bf16[2,4,4,96,256]{4,3,2,1,0:T(8,128)(2,1)} %collective-permute-done.9.refs_6_), channel_id=1, source_target_pairs={{0,32},{4,228},{32,64},{36,4},{64,96},{68,36},{96,128},{100,68},{1... | collective-permute-start | bytes 4718600 | tf_op jit(solution)/shard_map/ppermute | solution.py:310
  75.6 2.1 copy-start.3
  77.7 44.9 %collective-permute-start.22 = (bf16[2,4,8,96,256]{4,3,2,1,0:T(8,128)(2,1)}, bf16[2,4,8,96,256]{4,3,2,1,0:T(8,128)(2,1)S(1)}, u32[]{:S(2)}, u32[]{:S(2)}) collective-permute-start(bf16[2,4,8,96,256]{4,3,2,1,0:T(8,128)(2,1)} %pad_maximum_fusion), channel_id=1, source_target_pairs={{0,1},{4,7},{1,2},{5,4},{2,3},{6,5},{3,0},{7,6},{8,9},{12,15},{9,1... | collective-permute-start | bytes 9437192 | tf_op jit(solution)/shard_map/ppermute | solution.py:310
  78.8 2.2 copy-start.5
  81.0 41.8 %collective-permute-start.31 = (bf16[2,4,8,96,256]{4,3,2,1,0:T(8,128)(2,1)}, bf16[2,4,8,96,256]{4,3,2,1,0:T(8,128)(2,1)}, u32[]{:S(2)}, u32[]{:S(2)}) collective-permute-start(bf16[2,4,8,96,256]{4,3,2,1,0:T(8,128)(2,1)} %pad_maximum_fusion.1), channel_id=1, source_target_pairs={{0,8},{4,28},{8,16},{12,4},{16,24},{20,12},{24,0},{28,20},{1,9},{5... | collective-permute-start | bytes 9437192 | tf_op jit(solution)/shard_map/ppermute | solution.py:310
  97.5 21.9 %collective-permute-start.13 = (bf16[2,4,4,96,256]{4,3,2,1,0:T(8,128)(2,1)}, bf16[2,4,4,96,256]{4,3,2,1,0:T(8,128)(2,1)}, u32[]{:S(2)}, u32[]{:S(2)}) collective-permute-start(bf16[2,4,4,96,256]{4,3,2,1,0:T(8,128)(2,1)} %collective-permute-done.11.refs_8_), channel_id=1, source_target_pairs={{0,32},{4,228},{32,64},{36,4},{64,96},{68,36},{96,128},{100,68},{1... | collective-permute-start | bytes 4718600 | tf_op jit(solution)/shard_map/ppermute | solution.py:310
  97.5 31.1 %collective-permute-start.10 = (bf16[2,4,4,96,256]{4,3,2,1,0:T(8,128)(2,1)}, bf16[2,4,4,96,256]{4,3,2,1,0:T(8,128)(2,1)}, u32[]{:S(2)}, u32[]{:S(2)}) collective-permute-start(bf16[2,4,4,96,256]{4,3,2,1,0:T(8,128)(2,1)} %collective-permute-done.9.refs_6_), channel_id=1, source_target_pairs={{0,4},{4,0},{1,5},{5,1},{2,6},{6,2},{3,7},{7,3},{8,12},{12,8},{9,1... | collective-permute-start | bytes 4718600 | tf_op jit(solution)/shard_map/ppermute | solution.py:296
  97.5 32.6 %collective-permute-start.12 = (bf16[2,4,4,96,256]{4,3,2,1,0:T(8,128)(2,1)}, bf16[2,4,4,96,256]{4,3,2,1,0:T(8,128)(2,1)}, u32[]{:S(2)}, u32[]{:S(2)}) collective-permute-start(bf16[2,4,4,96,256]{4,3,2,1,0:T(8,128)(2,1)} %collective-permute-done.11.refs_8_), channel_id=1, source_target_pairs={{0,4},{4,0},{1,5},{5,1},{2,6},{6,2},{3,7},{7,3},{8,12},{12,8},{9,1... | collective-permute-start | bytes 4718600 | tf_op jit(solution)/shard_map/ppermute | solution.py:296
  119.4 6.1 %collective-permute-start = (bf16[96,512]{1,0:T(8,128)(2,1)S(1)}, bf16[96,512]{1,0:T(8,128)(2,1)S(1)}, u32[]{:S(2)}, u32[]{:S(2)}) collective-permute-start(bf16[96,512]{1,0:T(8,128)(2,1)S(1)} %slice.33), channel_id=1, source_target_pairs={{0,4},{4,8},{8,12},{12,16},{16,20},{20,24},{24,28},{28,32},{32,36}... | collective-permute-start | bytes 294920 | tf_op jit(solution)/shard_map/ppermute | solution.py:324
  122.6 6.1 %copy-start.1 = (bf16[2,4,8,96,256]{4,3,2,1,0:T(8,128)(2,1)}, bf16[2,4,8,96,256]{4,3,2,1,0:T(8,128)(2,1)S(1)}, u32[]{:S(2)}) copy-start(bf16[2,4,8,96,256]{4,3,2,1,0:T(8,128)(2,1)S(1)} %collective-permute-done.22.refs_6_) | copy-start | bytes 9437188
  122.6 13.3 %collective-permute-start.15 = (bf16[2,2,4,96,256]{4,3,2,1,0:T(8,128)(2,1)S(1)}, bf16[2,2,4,96,256]{4,3,2,1,0:T(8,128)(2,1)S(1)}, u32[]{:S(2)}, u32[]{:S(2)}) collective-permute-start(bf16[2,2,4,96,256]{4,3,2,1,0:T(8,128)(2,1)S(1)} %constant_dynamic-slice_fusion.2), channel_id=1, source_target_pairs={{0,32},{4,228},{32,64},{36,4},{64,96},{68,36},{96,128},{100,68},{1... | collective-permute-start | bytes 2359304 | tf_op jit(solution)/shard_map/ppermute | solution.py:310
  122.8 26.6 %copy-start.14 = (f32[3,256]{1,0:T(4,128)S(1)}, f32[3,256]{1,0:T(4,128)}, u32[]{:S(2)}) copy-start(f32[3,256]{1,0:T(4,128)} %param.14) | copy-start | bytes 9220
  122.8 26.6 %copy-start.15 = (f32[3,256]{1,0:T(4,128)S(1)}, f32[3,256]{1,0:T(4,128)}, u32[]{:S(2)}) copy-start(f32[3,256]{1,0:T(4,128)} %param.13) | copy-start | bytes 9220
  122.8 26.6 %copy-start.11 = (f32[3,31,256]{2,1,0:T(8,128)S(1)}, f32[3,31,256]{2,1,0:T(8,128)}, u32[]{:S(2)}) copy-start(f32[3,31,256]{2,1,0:T(8,128)} %param.12) | copy-start | bytes 285700
  122.8 21.8 %collective-permute-start.24 = (bf16[2,2,8,96,256]{4,3,2,1,0:T(8,128)(2,1)S(1)}, bf16[2,2,8,96,256]{4,3,2,1,0:T(8,128)(2,1)}, u32[]{:S(2)}, u32[]{:S(2)}) collective-permute-start(bf16[2,2,8,96,256]{4,3,2,1,0:T(8,128)(2,1)S(1)} %constant_dynamic-slice_fusion.1), channel_id=1, source_target_pairs={{0,1},{4,7},{1,2},{5,4},{2,3},{6,5},{3,0},{7,6},{8,9},{12,15},{9,1... | collective-permute-start | bytes 4718600 | tf_op jit(solution)/shard_map/ppermute | solution.py:310
  125.6 28.9 %copy-start.13 = (f32[3,2048]{1,0:T(4,128)S(1)}, f32[3,2048]{1,0:T(4,128)}, u32[]{:S(2)}) copy-start(f32[3,2048]{1,0:T(4,128)} %param.9) | copy-start | bytes 73732
  125.6 30.2 %copy-start.12 = (bf16[96,512]{1,0:T(8,128)(2,1)}, bf16[96,512]{1,0:T(8,128)(2,1)S(1)}, u32[]{:S(2)}) copy-start(bf16[96,512]{1,0:T(8,128)(2,1)S(1)} %collective-permute-done.before_ref) | copy-start | bytes 294916
  125.6 21.0 %collective-permute-start.33 = (bf16[2,2,8,96,256]{4,3,2,1,0:T(8,128)(2,1)S(1)}, bf16[2,2,8,96,256]{4,3,2,1,0:T(8,128)(2,1)}, u32[]{:S(2)}, u32[]{:S(2)}) collective-permute-start(bf16[2,2,8,96,256]{4,3,2,1,0:T(8,128)(2,1)S(1)} %constant_dynamic-slice_fusion), channel_id=1, source_target_pairs={{0,8},{4,28},{8,16},{12,4},{16,24},{20,12},{24,0},{28,20},{1,9},{5... | collective-permute-start | bytes 4718600 | tf_op jit(solution)/shard_map/ppermute | solution.py:310
  128.6 67.9 %collective-permute-start.23 = (bf16[2,4,8,96,256]{4,3,2,1,0:T(8,128)(2,1)S(1)}, bf16[2,4,8,96,256]{4,3,2,1,0:T(8,128)(2,1)}, u32[]{:S(2)}, u32[]{:S(2)}) collective-permute-start(bf16[2,4,8,96,256]{4,3,2,1,0:T(8,128)(2,1)S(1)} %collective-permute-done.22.refs_6_), channel_id=1, source_target_pairs={{0,4},{4,0},{1,5},{5,1},{2,6},{6,2},{3,7},{7,3},{8,12},{12,8},{9,1... | collective-permute-start | bytes 9437192 | tf_op jit(solution)/shard_map/ppermute | solution.py:296
  130.1 66.4 %collective-permute-start.32 = (bf16[2,4,8,96,256]{4,3,2,1,0:T(8,128)(2,1)}, bf16[2,4,8,96,256]{4,3,2,1,0:T(8,128)(2,1)}, u32[]{:S(2)}, u32[]{:S(2)}) collective-permute-start(bf16[2,4,8,96,256]{4,3,2,1,0:T(8,128)(2,1)} %collective-permute-done.31.refs_12_), channel_id=1, source_target_pairs={{0,4},{4,0},{1,5},{5,1},{2,6},{6,2},{3,7},{7,3},{8,12},{12,8},{9,1... | collective-permute-start | bytes 9437192 | tf_op jit(solution)/shard_map/ppermute | solution.py:296
  135.9 10.8 %copy-start.7 = (bf16[2,2,4,96,256]{4,3,2,1,0:T(8,128)(2,1)}, bf16[2,2,4,96,256]{4,3,2,1,0:T(8,128)(2,1)S(1)}, u32[]{:S(2)}) copy-start(bf16[2,2,4,96,256]{4,3,2,1,0:T(8,128)(2,1)S(1)} %collective-permute-done.15.refs_12_) | copy-start | bytes 2359300
  135.9 18.5 %collective-permute-start.14 = (bf16[2,4,4,96,256]{4,3,2,1,0:T(8,128)(2,1)}, bf16[2,4,4,96,256]{4,3,2,1,0:T(8,128)(2,1)}, u32[]{:S(2)}, u32[]{:S(2)}) collective-permute-start(bf16[2,4,4,96,256]{4,3,2,1,0:T(8,128)(2,1)} %collective-permute-done.13.refs_10_), channel_id=1, source_target_pairs={{0,4},{4,0},{1,5},{5,1},{2,6},{6,2},{3,7},{7,3},{8,12},{12,8},{9,1... | collective-permute-start | bytes 4718600 | tf_op jit(solution)/shard_map/ppermute | solution.py:296
  144.6 51.9 %collective-permute-start.25 = (bf16[2,2,8,96,256]{4,3,2,1,0:T(8,128)(2,1)}, bf16[2,2,8,96,256]{4,3,2,1,0:T(8,128)(2,1)}, u32[]{:S(2)}, u32[]{:S(2)}) collective-permute-start(bf16[2,2,8,96,256]{4,3,2,1,0:T(8,128)(2,1)} %collective-permute-done.24.refs_8_), channel_id=1, source_target_pairs={{0,4},{4,0},{1,5},{5,1},{2,6},{6,2},{3,7},{7,3},{8,12},{12,8},{9,1... | collective-permute-start | bytes 4718600 | tf_op jit(solution)/shard_map/ppermute | solution.py:296
  146.6 49.9 %collective-permute-start.34 = (bf16[2,2,8,96,256]{4,3,2,1,0:T(8,128)(2,1)}, bf16[2,2,8,96,256]{4,3,2,1,0:T(8,128)(2,1)}, u32[]{:S(2)}, u32[]{:S(2)}) collective-permute-start(bf16[2,2,8,96,256]{4,3,2,1,0:T(8,128)(2,1)} %collective-permute-done.33.refs_14_), channel_id=1, source_target_pairs={{0,4},{4,0},{1,5},{5,1},{2,6},{6,2},{3,7},{7,3},{8,12},{12,8},{9,1... | collective-permute-start | bytes 4718600 | tf_op jit(solution)/shard_map/ppermute | solution.py:296
  150.2 13.8 %all-to-all-start.1 = ((f32[4,3,33,256]{3,2,1,0:T(8,128)}), f32[4,3,33,256]{3,2,1,0:T(8,128)}, u32[]{:S(2)}, u32[]{:S(2)}) async-start(f32[4,3,33,256]{3,2,1,0:T(8,128)} %broadcast_in_dim.14), calls=%async_computation.1 | async-start | bytes 983040 | tf_op jit(solution)/shard_map/all_to_all | solution.py:273
  154.4 27.2 %collective-permute-start.16 = (bf16[2,2,4,96,256]{4,3,2,1,0:T(8,128)(2,1)}, bf16[2,2,4,96,256]{4,3,2,1,0:T(8,128)(2,1)}, u32[]{:S(2)}, u32[]{:S(2)}) collective-permute-start(bf16[2,2,4,96,256]{4,3,2,1,0:T(8,128)(2,1)} %copy-done.7), channel_id=1, source_target_pairs={{0,4},{4,0},{1,5},{5,1},{2,6},{6,2},{3,7},{7,3},{8,12},{12,8},{9,1... | collective-permute-start | bytes 2359304 | tf_op jit(solution)/shard_map/ppermute | solution.py:296
where the time goes:
time: 234 us; the launch traced here: 229 us
  waiting for transfers between devices  93.1 us (40%)
  starting transfers between devices  52 us (22%)
  Pallas kernels  39 us (17%)
  blocking collectives  29.1 us (12%)
  local copies, waits for them, and re-layouts  9.02 us (4%)
  other arithmetic  6.28 us (3%)
    ppermute x8, waiting for transfers between devices, last_parts(): moving = lax.ppermute(moving, axes, route)  64.6 us
    pallas_call x2, Pallas kernels, modules(): pl.pallas_call(functools.partial(modules_kernel, first, [len(p) for p in...  35 us
    ppermute x15, waiting for transfers between devices, shift(): return lax.ppermute(a, axis, [(i, (i + by) % n) for i in range(n)])  24.2 us
    ppermute x15, starting transfers between devices, shift(): return lax.ppermute(a, axis, [(i, (i + by) % n) for i in range(n)])  21.8 us
    all_to_all x1, blocking collectives, shards(): lax.all_to_all(windows, 'y', 0, 0, tiled=True)  17.6 us
    all_to_all x2, starting transfers between devices, to_each(): lax.all_to_all(jnp.broadcast_to(a, (SPAN[axis], *a.shape)), axis, 0, 0, t...  12.6 us
    all_to_all x1, blocking collectives, shards(): return lax.all_to_all(x, 'y', 0, 0, tiled=True).reshape(inputs.shape)  11.5 us
    ppermute x8, starting transfers between devices, last_parts(): moving = lax.ppermute(moving, axes, route)  9.01 us
  transfers between devices with their start and end apart: 37, of which 16 were waited for; matrix products, arithmetic and copies ran while one was open for 5% of the time, Pallas kernels for 8%

commit v1 on v0

--- a/solution.py
+++ b/solution.py
@@ -10,7 +10,7 @@
 
 NZ, NX, NC, NY = 8, 4, 2, 4
 HALO = 32
-ROWS = 64
+ROWS = 32
 TILE = 8
 DEPTH, WIDE = 32, 256
 GROUP = NX * NC * DEPTH
@@ -54,10 +54,14 @@
             pad_ref[lead + k * rows : lead + (k + 1) * rows] = turned.astype(jnp.bfloat16)
         for k in range(count):
             windows_ref[k, half] = pad_ref[k * rows : k * rows + window]
-    for layer in range(gain_ref.shape[0]):
-        for d in range(NZ):
-            row = gain_ref[layer, pl.ds((at_z + d) % NZ, 1), :]
-            rel_ref[layer, d : d + 1, :] = to_relative(jnp.broadcast_to(row, (8, group)), at_x, core)[:1]
+
+    def turned_gain(i, carry):
+        layer, d = i // NZ, i % NZ
+        row = gain_ref[layer, pl.ds((at_z + d) % NZ, 1), :]
+        rel_ref[layer, pl.ds(d, 1), :] = to_relative(jnp.broadcast_to(row, (8, group)), at_x, core)[:1]
+        return carry
+
+    lax.fori_loop(0, gain_ref.shape[0] * NZ, turned_gain, 0)
 
 
 def prepare(info, before, x, gain):
@@ -86,16 +90,19 @@
             [shard(kind, dy, dz, dx, dc) for dz in zs for dx in range(NX) for dc in range(NC)], axis=0
         )
 
-    total = jnp.zeros((rows_in, 1), jnp.float32)
-    for dz in range(NZ):
+    def squares(dz, total):
         xf = x_of(dz).astype(jnp.float32)
-        total = total + jnp.sum(xf * xf, axis=1, keepdims=True)
+        return total + jnp.sum(xf * xf, axis=1, keepdims=True)
+
+    total = lax.fori_loop(0, NZ, squares, jnp.zeros((rows_in, 1), jnp.float32))
     scale = lax.rsqrt(total / (NZ * GROUP) + 1e-06)
-    for dz in range(NZ):
-        xf = x_of(dz).astype(jnp.float32)
-        hid_ref[:rows_in, dz * GROUP : (dz + 1) * GROUP] = (xf * scale * gain_ref[layer, dz : dz + 1, :]).astype(
-            jnp.bfloat16
-        )
+
+    def normalised(dz, carry):
+        h = x_of(dz).astype(jnp.float32) * scale * gain_ref[layer, pl.ds(dz, 1), :]
+        hid_ref[:rows_in, pl.ds(pl.multiple_of(dz * GROUP, GROUP), GROUP)] = h.astype(jnp.bfloat16)
+        return carry
+
+    lax.fori_loop(0, NZ, normalised, 0)
 
     lead = HALO - reach
     row = lax.broadcasted_iota(jnp.int32, (rows_in, 1), 0)
@@ -116,18 +123,22 @@
         gate = jnp.dot(hidden, matrix(1, dy, range(NZ)), preferred_element_type=jnp.float32)
         glu = (value * jax.nn.sigmoid(gate)).astype(jnp.bfloat16).astype(jnp.float32)
         glu_ref[:rows_in] = jnp.where(ahead, 0.0, glu)
-        for r in range(0, rows, ROWS):
-            count = min(ROWS, rows - r)
-            acc = jnp.zeros((count, WIDE), jnp.float32)
+
+        def filtered(i, carry):
+            r = pl.multiple_of(i * ROWS, ROWS)
+            acc = jnp.zeros((ROWS, WIDE), jnp.float32)
             for s in range(TILE):
                 extra = TILE if s else 0
-                part = jnp.zeros((count + extra, WIDE), jnp.float32)
+                part = jnp.zeros((ROWS + extra, WIDE), jnp.float32)
                 for tap in range(reach + 1):
                     if (tap + lead) % TILE == s:
-                        at = r + tap + lead - s
-                        part = part + small_of(dy, layer, tap) * glu_ref[at : at + count + extra, :]
-                acc = acc + part[s : s + count]
-            fil_ref[dy, r : r + count, :] = acc
+                        at = pl.multiple_of(r + (tap + lead - s), TILE)
+                        part = part + small_of(dy, layer, tap) * glu_ref[pl.ds(at, ROWS + extra), :]
+                acc = acc + part[s : s + ROWS]
+            fil_ref[dy, pl.ds(r, ROWS), :] = acc
+            return carry
+
+        lax.fori_loop(0, rows // ROWS, filtered, 0)
         return carry
 
     lax.fori_loop(0, NY, block, 0)
@@ -140,9 +151,14 @@
         square = square + jnp.sum(f * f, axis=1, keepdims=True)
     mean = total / channels
     scale = lax.rsqrt(square / channels - mean * mean + 1e-06)
-    for dy in range(NY):
+
+    def activated(dy, carry):
         v = (fil_ref[dy, :rows] - mean) * scale * small_of(dy, layer, reach + 1) + small_of(dy, layer, reach + 2)
-        norm_ref[:rows, dy * WIDE : (dy + 1) * WIDE] = (v * jax.nn.sigmoid(v)).astype(jnp.bfloat16)
+        cols = pl.ds(pl.multiple_of(dy * WIDE, WIDE), WIDE)
+        norm_ref[:rows, cols] = (v * jax.nn.sigmoid(v)).astype(jnp.bfloat16)
+        return carry
+
+    lax.fori_loop(0, NY, activated, 0)
 
     def features(dz, carry):
         weight = jnp.concatenate([matrix(2, dy, (dz,)) for dy in range(NY)], axis=1)
@@ -157,20 +173,16 @@
 
 def copies_of(plan, part_refs, held_ref, core, sems):
     n = SPAN[plan["last"]]
-    half = held_ref.shape[2] // 2
-    pairs = [[(part_refs[0], held_ref.at[0, 0]), (part_refs[1], held_ref.at[0, 1])]]
-    for k in range(1, n // 2 + 1):
-        mine, other = part_refs[2 * k : 2 * k + 2]
+    groups = [[(part_refs[0], 0, 0), (part_refs[1], 0, 1)]]
+    rest = list(part_refs[2:])
+    for k in range(1, n // 2):
         here = jnp.where(core == 0, n - k, k)
-        there = n - here
-        if k < n // 2:
-            to = lambda d, c: held_ref.at[d, c]
-        else:
-            here, there = core, 1 - core
-            to = lambda d, c, k=k: held_ref.at[k, c, pl.ds(d * half, half)]
-        pairs.append(
-            [(part.at[c], to(d, c ^ swap)) for part, d, swap in ((mine, here, 0), (other, there, 1)) for c in range(NC)]
+        mine, other, rest = rest[:2], rest[2:4], rest[4:]
+        groups.append(
+            [(mine[0], here, 0), (mine[1], here, 1), (other[0], n - here, 1), (other[1], n - here, 0)]
         )
+    groups.append([(rest[0], n // 2, 0), (rest[1], n // 2, 1)])
+    pairs = [[(ref, held_ref.at[d, c]) for ref, d, c in group] for group in groups]
     if plan["last"] != "y":
         pairs = [[pair for group in pairs for pair in group]]
     count = iter(range(sems.shape[0]))
@@ -254,7 +266,7 @@
             for p in plans
         ]
         + [
-            pltpu.SemaphoreType.DMA((2 * len(p) - 2,)) for p in parts
+            pltpu.SemaphoreType.DMA((2 * NZ,)) for p in parts
         ],
         cost_estimate=pl.CostEstimate(
             flops=len(parts) * 6 * rows_in * 2048 * 1024,
@@ -296,20 +308,23 @@
     return lax.ppermute(a, "c", [(0, 1), (1, 0)])
 
 
-def last_parts(block, axis, core):
+def last_parts(block, axis):
     n = SPAN[axis]
-    parts = [block, swapped(block)]
-    moving = jnp.stack(parts)
     axes = ("c", "y") if axis == "y" else (axis, "c")
     at = lambda i, c: c * n + i if axis == "y" else i * NC + c
     route = [(at(i, c), at((i + 1 - 2 * c) % n, c)) for i in range(n) for c in range(NC)]
-    for k in range(1, n // 2 + 1):
-        if k == n // 2:
-            half = block.shape[0] // 2
-            moving = lax.dynamic_slice_in_dim(moving, core * half, half, 1)
-        moving = lax.ppermute(moving, axes, route)
-        parts += [moving, swapped(moving)]
-    return parts
+
+    def sent(a):
+        return lax.ppermute(a, axes, route)
+
+    other = swapped(block)
+    parts = [block, other]
+    own = block
+    for _ in range(1, n // 2):
+        own, other = sent(own), sent(other)
+        parts += [own, other, swapped(own), swapped(other)]
+    own = sent(own)
+    return [*parts, own, swapped(own)]
 
 
 def shards(inputs, norm_gain, w_value, w_gate, conv_taps, ln_gain, ln_bias, w_out):
@@ -327,17 +342,17 @@
     own = jnp.concatenate((conv_taps, ln_gain[:, None], ln_bias[:, None]), axis=1)
     small = to_each(own, "y")
     packed = jnp.concatenate((w_value, w_gate, jnp.swapaxes(w_out, 1, 2)), axis=1)
-    alone = packed[0]
-    xs = jnp.stack([alone, shift(alone, "x", -1), shift(alone, "x", 2), shift(alone, "x", 1)])
+    xs = to_each(packed[0], "x")
+    xs = lax.dynamic_slice_in_dim(jnp.concatenate((xs, xs)), at_x, NX)
     zs = to_each(packed[1:], "z")
-    block0 = gathered(xs, "y")
+    block0 = jnp.stack([xs, shift(xs, "y", -1), shift(xs, "y", 2), shift(xs, "y", 1)])
     block0, zs = lax.optimization_barrier((block0, zs))
     zs = lax.dynamic_slice_in_dim(jnp.concatenate((zs, zs)), at_z, NZ)
     block1 = gathered(zs[:, 0], "x")
     block2 = gathered(zs[:, 1], "y")
-    parts0 = last_parts(block0, "z", core)
-    parts1 = last_parts(block1, "y", core)
-    parts2 = last_parts(block2, "x", core)
+    parts0 = last_parts(block0, "z")
+    parts1 = last_parts(block1, "y")
+    parts2 = last_parts(block2, "x")
     x = modules(info, x, gain, small, [parts0], 0)
     x = modules(info, x, gain, small, [parts1, parts2], 1)
     return lax.all_to_all(x, "y", 0, 0, tiled=True).reshape(inputs.shape)

time: 234 us -> 249 us (1.064); the launches traced: 229 us -> 248 us
  waiting for transfers between devices: 93.1 us -> 116 us
  Pallas kernels: 39 us -> 44.2 us
  starting transfers between devices: 52 us -> 48.9 us
  other arithmetic: 6.28 us -> 3.46 us
    ppermute x8 -> x13, waiting for transfers between devices: 64.6 us -> 87 us  [sent(): return lax.ppermute(a, axes, route)]
    ppermute x15 -> x11, waiting for transfers between devices: 24.2 us -> 17.1 us  [shift(): return lax.ppermute(a, axis, [(i, (i + by) % n) for i in range(n)])]
    all_to_all x2 -> x3, waiting for transfers between devices: 4.26 us -> 11.3 us  [to_each(): lax.all_to_all(jnp.broadcast_to(a, (SPAN[axis], *a.shape)), axis, 0, 0, t...]
    all_to_all x2 -> x3, starting transfers between devices: 12.6 us -> 18.2 us  [to_each(): lax.all_to_all(jnp.broadcast_to(a, (SPAN[axis], *a.shape)), axis, 0, 0, t...]
    ppermute x15 -> x11, starting transfers between devices: 21.8 us -> 16.9 us  [shift(): return lax.ppermute(a, axis, [(i, (i + by) % n) for i in range(n)])]
    another operation x5 -> x2, other arithmetic: 4.91 us -> 1.06 us  [shards(): jnp.stack([xs, shift(xs, 'y', -1), shift(xs, 'y', 2), shift(xs, 'y', 1)])]
    dynamic_slice x3 -> x0, local copies, waits for them, and re-layouts: 2.82 us -> none  [last_parts(): moving = lax.dynamic_slice_in_dim(moving, core * half, half, 1)]
    pallas_call x1, Pallas kernels: 4 us -> 6.65 us  [prepare(): pl.pallas_call(prepare_kernel, in_specs=[pl.BlockSpec(memory_space=pltpu....]
  transfers between devices with their start and end apart: 37 -> 44, of which waited for: 16 -> 22; matrix products, arithmetic and copies ran while one was open for 5% -> 2% of each run, Pallas kernels for 8% -> 9%
where the time goes in v1:
time: 249 us; the launch traced here: 248 us
  waiting for transfers between devices  116 us (47%)
  starting transfers between devices  48.9 us (20%)
  Pallas kernels  44.2 us (18%)
  blocking collectives  28.9 us (12%)
  local copies, waits for them, and re-layouts  6.66 us (3%)
  other arithmetic  3.46 us (1%)
    ppermute x13, waiting for transfers between devices, sent(): return lax.ppermute(a, axes, route)  87 us
    pallas_call x2, Pallas kernels, modules(): pl.pallas_call(functools.partial(modules_kernel, first, [len(p) for p in...  37.5 us
    all_to_all x3, starting transfers between devices, to_each(): lax.all_to_all(jnp.broadcast_to(a, (SPAN[axis], *a.shape)), axis, 0, 0, t...  18.2 us
    all_to_all x1, blocking collectives, shards(): lax.all_to_all(windows, 'y', 0, 0, tiled=True)  17.4 us
    ppermute x11, waiting for transfers between devices, shift(): return lax.ppermute(a, axis, [(i, (i + by) % n) for i in range(n)])  17.1 us
    ppermute x11, starting transfers between devices, shift(): return lax.ppermute(a, axis, [(i, (i + by) % n) for i in range(n)])  16.9 us
    all_to_all x1, blocking collectives, shards(): return lax.all_to_all(x, 'y', 0, 0, tiled=True).reshape(inputs.shape)  11.5 us
    all_to_all x3, waiting for transfers between devices, to_each(): lax.all_to_all(jnp.broadcast_to(a, (SPAN[axis], *a.shape)), axis, 0, 0, t...  11.3 us
  transfers between devices with their start and end apart: 44, of which 22 were waited for; matrix products, arithmetic and copies ran while one was open for 2% of the time, Pallas kernels for 9%

profile of v1, /device:TPU:4, one launch (start us, length us, event | category | flops | bytes accessed | tf_op | source)
XLA Modules:
  0.0 248.1 jit_solution(17511048527439628660)
XLA Ops:
  0.0 0.8 maximum_bitcast_fusion.2
  0.8 0.7 broadcast_in_dim.18
  1.4 5.5 %all-to-all-start.2 = ((bf16[4,96,256]{2,1,0:T(8,128)(2,1)}), bf16[4,96,256]{2,1,0:T(8,128)(2,1)S(1)}, u32[]{:S(2)}, u32[]{:S(2)}) async-start(bf16[4,96,256]{2,1,0:T(8,128)(2,1)} %broadcast_in_dim.18), calls=%async_computation.2 | async-start | bytes 393216 | tf_op jit(solution)/shard_map/all_to_all | solution.py:285
  7.0 0.8 pad_maximum_fusion.4
  7.8 2.6 %all-to-all-done.2 = bf16[4,96,256]{2,1,0:T(8,128)(2,1)S(1)} async-done(((bf16[4,96,256]{2,1,0:T(8,128)(2,1)}), bf16[4,96,256]{2,1,0:T(8,128)(2,1)S(1)}, u32[]{:S(2)}, u32[]{:S(2)}) %all-to-all-start.2) | async-done | bytes 196640 | tf_op jit(solution)/shard_map/all_to_all | solution.py:285
  10.4 1.0 broadcast_in_dim.19
  11.4 7.7 %all-to-all-start.3 = ((bf16[8,2,96,256]{3,2,1,0:T(8,128)(2,1)}), bf16[8,2,96,256]{3,2,1,0:T(8,128)(2,1)S(1)}, u32[]{:S(2)}, u32[]{:S(2)}) async-start(bf16[8,2,96,256]{3,2,1,0:T(8,128)(2,1)} %broadcast_in_dim.19), calls=%async_computation.3 | async-start | bytes 1572864 | tf_op jit(solution)/shard_map/all_to_all | solution.py:285
  19.2 3.1 %collective-permute-start.1 = (bf16[4,96,256]{2,1,0:T(8,128)(2,1)S(1)}, bf16[4,96,256]{2,1,0:T(8,128)(2,1)S(1)}, u32[]{:S(2)}, u32[]{:S(2)}) collective-permute-start(bf16[4,96,256]{2,1,0:T(8,128)(2,1)S(1)} %fusion.1), channel_id=1, source_target_pairs={{0,3},{1,0},{2,1},{3,2},{4,7},{5,4},{6,5},{7,6},{8,11},{9,8},{10,9... | collective-permute-start | bytes 589832 | tf_op jit(solution)/shard_map/ppermute | solution.py:281
  22.3 0.6 collective-permute-start.2
  23.0 1.0 collective-permute-start.3
  24.0 5.0 %collective-permute-done.1 = bf16[4,96,256]{2,1,0:T(8,128)(2,1)S(1)} collective-permute-done((bf16[4,96,256]{2,1,0:T(8,128)(2,1)S(1)}, bf16[4,96,256]{2,1,0:T(8,128)(2,1)S(1)}, u32[]{:S(2)}, u32[]{:S(2)}) %collective-permute-start.1) | collective-permute-done | bytes 196640 | tf_op jit(solution)/shard_map/ppermute | solution.py:281
  29.0 1.6 collective-permute-done.2
  30.6 2.1 collective-permute-done.3
  32.7 1.0 pad_maximum_fusion.2.refs_4_
  33.7 7.2 %all-to-all-done.3 = bf16[8,2,96,256]{3,2,1,0:T(8,128)(2,1)S(1)} async-done(((bf16[8,2,96,256]{3,2,1,0:T(8,128)(2,1)}), bf16[8,2,96,256]{3,2,1,0:T(8,128)(2,1)S(1)}, u32[]{:S(2)}, u32[]{:S(2)}) %all-to-all-start.3) | async-done | bytes 786464 | tf_op jit(solution)/shard_map/all_to_all | solution.py:285
  40.8 0.7 collective-permute-start.5
  42.0 2.1 collective-permute-start.20
  44.2 1.6 collective-permute-start.31
  45.7 1.7 collective-permute-start.30
  47.4 3.4 %collective-permute-done.20 = bf16[8,96,256]{2,1,0:T(8,128)(2,1)S(1)} collective-permute-done((bf16[8,96,256]{2,1,0:T(8,128)(2,1)S(1)}, bf16[8,96,256]{2,1,0:T(8,128)(2,1)S(1)}, u32[]{:S(2)}, u32[]{:S(2)}) %collective-permute-start.20) | collective-permute-done | bytes 393248 | tf_op jit(solution)/shard_map/ppermute | solution.py:281
  50.8 3.5 %collective-permute-done.5.refs_6_ = bf16[4,4,96,256]{3,2,1,0:T(8,128)(2,1)S(1)} collective-permute-done((bf16[4,4,96,256]{3,2,1,0:T(8,128)(2,1)}, bf16[4,4,96,256]{3,2,1,0:T(8,128)(2,1)S(1)}, u32[]{:S(2)}, u32[]{:S(2)}) %collective-permute-start.5) | collective-permute-done | bytes 786464 | tf_op jit(solution)/shard_map/ppermute | solution.py:318
  54.3 2.1 collective-permute-start.21
  56.5 0.9 slice.27
  57.4 1.9 collective-permute-start
  59.4 0.7 collective-permute-done.21
  60.0 1.6 collective-permute-start.32
  61.6 1.3 collective-permute-done.22
  62.9 3.0 %collective-permute-start.33 = (bf16[4,96,256]{2,1,0:T(8,128)(2,1)S(1)}, bf16[4,96,256]{2,1,0:T(8,128)(2,1)S(1)}, u32[]{:S(2)}, u32[]{:S(2)}) collective-permute-start(bf16[4,96,256]{2,1,0:T(8,128)(2,1)S(1)} %slice.41), channel_id=1, source_target_pairs={{0,3},{1,0},{2,1},{3,2},{4,7},{5,4},{6,5},{7,6},{8,11},{9,8},{10,9... | collective-permute-start | bytes 589832 | tf_op jit(solution)/shard_map/ppermute | solution.py:281
  66.2 2.2 collective-permute-done.32
  68.3 0.4 collective-permute-start.24
  68.8 0.9 collective-permute-done.33
  69.8 1.0 collective-permute-start.7
  71.2 2.1 collective-permute-start.35
  73.3 0.6 collective-permute-start.6
  73.9 0.8 collective-permute-start.34
  74.7 13.2 %collective-permute-done.6.refs_7_ = bf16[4,4,96,256]{3,2,1,0:T(8,128)(2,1)S(1)} collective-permute-done((bf16[4,4,96,256]{3,2,1,0:T(8,128)(2,1)S(1)}, bf16[4,4,96,256]{3,2,1,0:T(8,128)(2,1)S(1)}, u32[]{:S(2)}, u32[]{:S(2)}) %collective-permute-start.6) | collective-permute-done | bytes 786464 | tf_op jit(solution)/shard_map/ppermute | solution.py:318
  87.9 2.1 collective-permute-done.24.refs_6_
  90.0 1.5 collective-permute-start.11
  91.5 0.3 collective-permute-done.35.refs_14_
  91.8 9.3 %collective-permute-done.13.refs_14_ = bf16[4,4,96,256]{3,2,1,0:T(8,128)(2,1)S(1)} collective-permute-done((bf16[4,4,96,256]{3,2,1,0:T(8,128)(2,1)S(1)}, bf16[4,4,96,256]{3,2,1,0:T(8,128)(2,1)S(1)}, u32[]{:S(2)}, u32[]{:S(2)}) %collective-permute-start.13) | collective-permute-done | bytes 786464 | tf_op jit(solution)/shard_map/ppermute | solution.py:318
  101.2 8.3 %collective-permute-done.10.refs_11_ = bf16[4,4,96,256]{3,2,1,0:T(8,128)(2,1)S(1)} collective-permute-done((bf16[4,4,96,256]{3,2,1,0:T(8,128)(2,1)S(1)}, bf16[4,4,96,256]{3,2,1,0:T(8,128)(2,1)S(1)}, u32[]{:S(2)}, u32[]{:S(2)}) %collective-permute-start.10) | collective-permute-done | bytes 786464 | tf_op jit(solution)/shard_map/ppermute | solution.py:318
  109.7 1.1 collective-permute-start.28
  110.9 7.0 %collective-permute-done.17.refs_18_ = bf16[4,4,96,256]{3,2,1,0:T(8,128)(2,1)S(1)} collective-permute-done((bf16[4,4,96,256]{3,2,1,0:T(8,128)(2,1)S(1)}, bf16[4,4,96,256]{3,2,1,0:T(8,128)(2,1)S(1)}, u32[]{:S(2)}, u32[]{:S(2)}) %collective-permute-start.17) | collective-permute-done | bytes 786464 | tf_op jit(solution)/shard_map/ppermute | solution.py:318
  118.0 1.1 collective-permute-start.25
  119.1 7.3 %collective-permute-done.14.refs_15_ = bf16[4,4,96,256]{3,2,1,0:T(8,128)(2,1)S(1)} collective-permute-done((bf16[4,4,96,256]{3,2,1,0:T(8,128)(2,1)S(1)}, bf16[4,4,96,256]{3,2,1,0:T(8,128)(2,1)S(1)}, u32[]{:S(2)}, u32[]{:S(2)}) %collective-permute-start.14) | collective-permute-done | bytes 786464 | tf_op jit(solution)/shard_map/ppermute | solution.py:318
  126.5 0.3 collective-permute-start.36
  126.8 5.1 %collective-permute-done.28.refs_10_ = bf16[4,8,96,256]{3,2,1,0:T(8,128)(2,1)} collective-permute-done((bf16[4,8,96,256]{3,2,1,0:T(8,128)(2,1)S(1)}, bf16[4,8,96,256]{3,2,1,0:T(8,128)(2,1)}, u32[]{:S(2)}, u32[]{:S(2)}) %collective-permute-start.28) | collective-permute-done | bytes 1572896 | tf_op jit(solution)/shard_map/ppermute | solution.py:318
  132.0 0.6 collective-permute-start.16
  132.6 16.3 %collective-permute-done.25.refs_7_ = bf16[4,8,96,256]{3,2,1,0:T(8,128)(2,1)} collective-permute-done((bf16[4,8,96,256]{3,2,1,0:T(8,128)(2,1)S(1)}, bf16[4,8,96,256]{3,2,1,0:T(8,128)(2,1)}, u32[]{:S(2)}, u32[]{:S(2)}) %collective-permute-start.25) | collective-permute-done | bytes 1572896 | tf_op jit(solution)/shard_map/ppermute | solution.py:318
  148.8 0.5 collective-permute-start.29
  149.3 14.7 %collective-permute-done.36.refs_15_ = bf16[4,8,96,256]{3,2,1,0:T(8,128)(2,1)} collective-permute-done((bf16[4,8,96,256]{3,2,1,0:T(8,128)(2,1)S(1)}, bf16[4,8,96,256]{3,2,1,0:T(8,128)(2,1)}, u32[]{:S(2)}, u32[]{:S(2)}) %collective-permute-start.36) | collective-permute-done | bytes 1572896 | tf_op jit(solution)/shard_map/ppermute | solution.py:318
  164.0 0.6 collective-permute-start.40
  164.9 0.7 copy-done.21
  165.6 0.8 broadcast_in_dim.17
  166.4 5.0 %all-to-all-start.1 = ((f32[4,3,33,256]{3,2,1,0:T(8,128)}), f32[4,3,33,256]{3,2,1,0:T(8,128)S(1)}, u32[]{:S(2)}, u32[]{:S(2)}) async-start(f32[4,3,33,256]{3,2,1,0:T(8,128)} %broadcast_in_dim.17), calls=%async_computation.1 | async-start | bytes 983040 | tf_op jit(solution)/shard_map/all_to_all | solution.py:285
  171.4 0.6 copy.21
  172.0 0.6 stack.74.info_ref.refs_0_
  172.6 6.6 %prepare.1 = (bf16[4,2,224,256]{3,2,1,0:T(8,128)(2,1)}, f32[3,8,256]{2,1,0:T(8,128)}) custom-call(s32[8]{0:T(128)} %stack.74.info_ref.refs_0_, bf16[96,512]{1,0:T(8,128)(2,1)} %copy-done.23, bf16[512,512]{1,0:T(8,128)(2,1)} %x_ref.1, f32[3,8,256]{2,1,0:T(8,128)} %bitcast.57), custom_call_target="tpu_custom_call" | custom-call | tf_op jit(solution)/shard_map/prepare/pallas_call | solution.py:70
  179.3 1.5 all-to-all-done.1.refs_3_
  180.8 17.4 %all_to_all.25 = bf16[4,2,224,256]{3,2,1,0:T(8,128)(2,1)} all-to-all(bf16[4,2,224,256]{3,2,1,0:T(8,128)(2,1)} %get-tuple-element.9), channel_id=1, replica_groups=mesh['z'=8,'x'=4,'c'=2,'y'=4] {'y'}, dimensions={0} | all-to-all | bytes 1835008 | tf_op jit(solution)/shard_map/all_to_all | solution.py:341
  198.2 15.7 %shard_map.82.refs_1_ = bf16[8,192,256]{2,1,0:T(8,128)(2,1)} custom-call(s32[8]{0:T(128)} %stack.74.info_ref.refs_0_, bf16[8,224,256]{2,1,0:T(8,128)(2,1)} %bitcast.46, f32[3,8,256]{2,1,0:T(8,128)} %get-tuple-element.10.refs_2_, f32[4,3,33,256]{3,2,1,0:T(8,128)} %copy-done.2, bf16[4,4,96,256]{3,2,1,0:T(8,128)(2,1)} %pad_maximum_fusion.2.refs_4_, ...), custom_call_target="tpu_custom_call" | custom-call | flops 2818572288 | bytes 12582912 | tf_op jit(solution)/shard_map/pallas_call | solution.py:250
  213.9 21.9 %shard_map.83 = bf16[4,128,512]{2,1,0:T(8,128)(2,1)} custom-call(s32[8]{0:T(128)} %stack.74.info_ref.refs_0_, bf16[8,192,256]{2,1,0:T(8,128)(2,1)} %shard_map.82.refs_1_, f32[3,8,256]{2,1,0:T(8,128)} %get-tuple-element.10.refs_2_, f32[4,3,33,256]{3,2,1,0:T(8,128)} %copy-done.2, bf16[4,8,96,256]{3,2,1,0:T(8,128)(2,1)} %copy-done, ...), custom_call_target="tpu_custom_call" | custom-call | flops 4831838208 | bytes 25165824 | tf_op jit(solution)/shard_map/pallas_call | solution.py:250
  235.8 11.5 %all_to_all.26 = bf16[4,128,512]{2,1,0:T(8,128)(2,1)S(1)} all-to-all(bf16[4,128,512]{2,1,0:T(8,128)(2,1)} %shard_map.83), channel_id=1, replica_groups=mesh['z'=8,'x'=4,'c'=2,'y'=4] {'y'}, dimensions={0} | all-to-all | bytes 1048576 | tf_op jit(solution)/shard_map/all_to_all | solution.py:358
  247.4 0.8 copy.23
  (108 shorter events, 2.3 us)
Async XLA Ops:
  1.4 9.0 %all-to-all-start.2 = ((bf16[4,96,256]{2,1,0:T(8,128)(2,1)}), bf16[4,96,256]{2,1,0:T(8,128)(2,1)S(1)}, u32[]{:S(2)}, u32[]{:S(2)}) async-start(bf16[4,96,256]{2,1,0:T(8,128)(2,1)} %broadcast_in_dim.18), calls=%async_computation.2 | async-start | bytes 393216 | tf_op jit(solution)/shard_map/all_to_all | solution.py:285
  11.4 29.4 %all-to-all-start.3 = ((bf16[8,2,96,256]{3,2,1,0:T(8,128)(2,1)}), bf16[8,2,96,256]{3,2,1,0:T(8,128)(2,1)S(1)}, u32[]{:S(2)}, u32[]{:S(2)}) async-start(bf16[8,2,96,256]{3,2,1,0:T(8,128)(2,1)} %broadcast_in_dim.19), calls=%async_computation.3 | async-start | bytes 1572864 | tf_op jit(solution)/shard_map/all_to_all | solution.py:285
  19.2 9.8 %collective-permute-start.1 = (bf16[4,96,256]{2,1,0:T(8,128)(2,1)S(1)}, bf16[4,96,256]{2,1,0:T(8,128)(2,1)S(1)}, u32[]{:S(2)}, u32[]{:S(2)}) collective-permute-start(bf16[4,96,256]{2,1,0:T(8,128)(2,1)S(1)} %fusion.1), channel_id=1, source_target_pairs={{0,3},{1,0},{2,1},{3,2},{4,7},{5,4},{6,5},{7,6},{8,11},{9,8},{10,9... | collective-permute-start | bytes 589832 | tf_op jit(solution)/shard_map/ppermute | solution.py:281
  22.3 8.3 %collective-permute-start.2 = (bf16[4,96,256]{2,1,0:T(8,128)(2,1)S(1)}, bf16[4,96,256]{2,1,0:T(8,128)(2,1)S(1)}, u32[]{:S(2)}, u32[]{:S(2)}) collective-permute-start(bf16[4,96,256]{2,1,0:T(8,128)(2,1)S(1)} %fusion.1), channel_id=1, source_target_pairs={{0,2},{1,3},{2,0},{3,1},{4,6},{5,7},{6,4},{7,5},{8,10},{9,11},{10,... | collective-permute-start | bytes 589832 | tf_op jit(solution)/shard_map/ppermute | solution.py:281
  23.0 9.7 %collective-permute-start.3 = (bf16[4,96,256]{2,1,0:T(8,128)(2,1)S(1)}, bf16[4,96,256]{2,1,0:T(8,128)(2,1)S(1)}, u32[]{:S(2)}, u32[]{:S(2)}) collective-permute-start(bf16[4,96,256]{2,1,0:T(8,128)(2,1)S(1)} %fusion.1), channel_id=1, source_target_pairs={{0,1},{1,2},{2,3},{3,0},{4,5},{5,6},{6,7},{7,4},{8,9},{9,10},{10,1... | collective-permute-start | bytes 589832 | tf_op jit(solution)/shard_map/ppermute | solution.py:281
  40.8 13.4 %collective-permute-start.5 = (bf16[4,4,96,256]{3,2,1,0:T(8,128)(2,1)}, bf16[4,4,96,256]{3,2,1,0:T(8,128)(2,1)S(1)}, u32[]{:S(2)}, u32[]{:S(2)}) collective-permute-start(bf16[4,4,96,256]{3,2,1,0:T(8,128)(2,1)} %pad_maximum_fusion.2.refs_4_), channel_id=1, source_target_pairs={{0,32},{4,228},{32,64},{36,4},{64,96},{68,36},{96,128},{100,68},{1... | collective-permute-start | bytes 2359304 | tf_op jit(solution)/shard_map/ppermute | solution.py:318
  42.0 8.8 %collective-permute-start.20 = (bf16[8,96,256]{2,1,0:T(8,128)(2,1)S(1)}, bf16[8,96,256]{2,1,0:T(8,128)(2,1)S(1)}, u32[]{:S(2)}, u32[]{:S(2)}) collective-permute-start(bf16[8,96,256]{2,1,0:T(8,128)(2,1)S(1)} %get-tuple-element.16), channel_id=1, source_target_pairs={{0,8},{8,16},{16,24},{24,0},{1,9},{9,17},{17,25},{25,1},{2,10},{10... | collective-permute-start | bytes 1179656 | tf_op jit(solution)/shard_map/ppermute | solution.py:281
  44.0 10.2 %collective-permute-start.19 = (bf16[8,96,256]{2,1,0:T(8,128)(2,1)S(1)}, bf16[8,96,256]{2,1,0:T(8,128)(2,1)S(1)}, u32[]{:S(2)}, u32[]{:S(2)}) collective-permute-start(bf16[8,96,256]{2,1,0:T(8,128)(2,1)S(1)} %get-tuple-element.16), channel_id=1, source_target_pairs={{0,24},{8,0},{16,8},{24,16},{1,25},{9,1},{17,9},{25,17},{2,26},{10... | collective-permute-start | bytes 1179656 | tf_op jit(solution)/shard_map/ppermute | solution.py:281
  44.2 12.2 %collective-permute-start.31 = (bf16[8,96,256]{2,1,0:T(8,128)(2,1)S(1)}, bf16[8,96,256]{2,1,0:T(8,128)(2,1)S(1)}, u32[]{:S(2)}, u32[]{:S(2)}) collective-permute-start(bf16[8,96,256]{2,1,0:T(8,128)(2,1)S(1)} %get-tuple-element.15), channel_id=1, source_target_pairs={{0,1},{1,2},{2,3},{3,0},{4,5},{5,6},{6,7},{7,4},{8,9},{9,10},{10,1... | collective-permute-start | bytes 1179656 | tf_op jit(solution)/shard_map/ppermute | solution.py:281
  45.7 11.7 %collective-permute-start.30 = (bf16[8,96,256]{2,1,0:T(8,128)(2,1)S(1)}, bf16[8,96,256]{2,1,0:T(8,128)(2,1)S(1)}, u32[]{:S(2)}, u32[]{:S(2)}) collective-permute-start(bf16[8,96,256]{2,1,0:T(8,128)(2,1)S(1)} %get-tuple-element.15), channel_id=1, source_target_pairs={{0,3},{1,0},{2,1},{3,2},{4,7},{5,4},{6,5},{7,6},{8,11},{9,8},{10,9... | collective-permute-start | bytes 1179656 | tf_op jit(solution)/shard_map/ppermute | solution.py:281
  50.8 20.4 %collective-permute-start.4 = (bf16[4,4,96,256]{3,2,1,0:T(8,128)(2,1)}, bf16[4,4,96,256]{3,2,1,0:T(8,128)(2,1)S(1)}, u32[]{:S(2)}, u32[]{:S(2)}) collective-permute-start(bf16[4,4,96,256]{3,2,1,0:T(8,128)(2,1)} %pad_maximum_fusion.2.refs_4_), channel_id=1, source_target_pairs={{0,4},{4,0},{1,5},{5,1},{2,6},{6,2},{3,7},{7,3},{8,12},{12,8},{9,1... | collective-permute-start | bytes 2359304 | tf_op jit(solution)/shard_map/ppermute | solution.py:308
  54.3 19.0 %collective-permute-start.9 = (bf16[4,4,96,256]{3,2,1,0:T(8,128)(2,1)S(1)}, bf16[4,4,96,256]{3,2,1,0:T(8,128)(2,1)S(1)}, u32[]{:S(2)}, u32[]{:S(2)}) collective-permute-start(bf16[4,4,96,256]{3,2,1,0:T(8,128)(2,1)S(1)} %collective-permute-done.5.refs_6_), channel_id=1, source_target_pairs={{0,32},{4,228},{32,64},{36,4},{64,96},{68,36},{96,128},{100,68},{1... | collective-permute-start | bytes 2359304 | tf_op jit(solution)/shard_map/ppermute | solution.py:318
  54.3 5.7 %collective-permute-start.21 = (bf16[4,96,256]{2,1,0:T(8,128)(2,1)S(1)}, bf16[4,96,256]{2,1,0:T(8,128)(2,1)S(1)}, u32[]{:S(2)}, u32[]{:S(2)}) collective-permute-start(bf16[4,96,256]{2,1,0:T(8,128)(2,1)S(1)} %slice.37), channel_id=1, source_target_pairs={{0,8},{8,16},{16,24},{24,0},{1,9},{9,17},{17,25},{25,1},{2,10},{10... | collective-permute-start | bytes 589832 | tf_op jit(solution)/shard_map/ppermute | solution.py:281
  56.4 6.5 %collective-permute-start.22 = (bf16[4,96,256]{2,1,0:T(8,128)(2,1)S(1)}, bf16[4,96,256]{2,1,0:T(8,128)(2,1)S(1)}, u32[]{:S(2)}, u32[]{:S(2)}) collective-permute-start(bf16[4,96,256]{2,1,0:T(8,128)(2,1)S(1)} %slice.38), channel_id=1, source_target_pairs={{0,24},{8,0},{16,8},{24,16},{1,25},{9,1},{17,9},{25,17},{2,26},{10... | collective-permute-start | bytes 589832 | tf_op jit(solution)/shard_map/ppermute | solution.py:281
  57.4 13.6 %collective-permute-start = (bf16[96,512]{1,0:T(8,128)(2,1)S(1)}, bf16[96,512]{1,0:T(8,128)(2,1)S(1)}, u32[]{:S(2)}, u32[]{:S(2)}) collective-permute-start(bf16[96,512]{1,0:T(8,128)(2,1)S(1)} %slice.27), channel_id=1, source_target_pairs={{0,4},{4,8},{8,12},{12,16},{16,20},{20,24},{24,28},{28,32},{32,36}... | collective-permute-start | bytes 294920 | tf_op jit(solution)/shard_map/ppermute | solution.py:339
  60.0 8.3 %collective-permute-start.32 = (bf16[4,96,256]{2,1,0:T(8,128)(2,1)S(1)}, bf16[4,96,256]{2,1,0:T(8,128)(2,1)S(1)}, u32[]{:S(2)}, u32[]{:S(2)}) collective-permute-start(bf16[4,96,256]{2,1,0:T(8,128)(2,1)S(1)} %slice.40), channel_id=1, source_target_pairs={{0,1},{1,2},{2,3},{3,0},{4,5},{5,6},{6,7},{7,4},{8,9},{9,10},{10,1... | collective-permute-start | bytes 589832 | tf_op jit(solution)/shard_map/ppermute | solution.py:281
  62.9 6.8 %collective-permute-start.33 = (bf16[4,96,256]{2,1,0:T(8,128)(2,1)S(1)}, bf16[4,96,256]{2,1,0:T(8,128)(2,1)S(1)}, u32[]{:S(2)}, u32[]{:S(2)}) collective-permute-start(bf16[4,96,256]{2,1,0:T(8,128)(2,1)S(1)} %slice.41), channel_id=1, source_target_pairs={{0,3},{1,0},{2,1},{3,2},{4,7},{5,4},{6,5},{7,6},{8,11},{9,8},{10,9... | collective-permute-start | bytes 589832 | tf_op jit(solution)/shard_map/ppermute | solution.py:281
  68.3 21.6 %collective-permute-start.24 = (bf16[4,8,96,256]{3,2,1,0:T(8,128)(2,1)S(1)}, bf16[4,8,96,256]{3,2,1,0:T(8,128)(2,1)S(1)}, u32[]{:S(2)}, u32[]{:S(2)}) collective-permute-start(bf16[4,8,96,256]{3,2,1,0:T(8,128)(2,1)S(1)} %pad_maximum_fusion.refs_4_), channel_id=1, source_target_pairs={{0,1},{4,7},{1,2},{5,4},{2,3},{6,5},{3,0},{7,6},{8,9},{12,15},{9,1... | collective-permute-start | bytes 4718600 | tf_op jit(solution)/shard_map/ppermute | solution.py:318
  69.8 4.1 %collective-permute-start.7 = (bf16[4,4,96,256]{3,2,1,0:T(8,128)(2,1)S(1)}, bf16[4,4,96,256]{3,2,1,0:T(8,128)(2,1)S(1)}, u32[]{:S(2)}, u32[]{:S(2)}) collective-permute-start(bf16[4,4,96,256]{3,2,1,0:T(8,128)(2,1)S(1)} %collective-permute-done.5.refs_6_), channel_id=1, source_target_pairs={{0,4},{4,0},{1,5},{5,1},{2,6},{6,2},{3,7},{7,3},{8,12},{12,8},{9,1... | collective-permute-start | bytes 2359304 | tf_op jit(solution)/shard_map/ppermute | solution.py:308
  70.8 94.8 %copy-start.25 = (f32[3,256]{1,0:T(4,128)S(1)}, f32[3,256]{1,0:T(4,128)}, u32[]{:S(2)}) copy-start(f32[3,256]{1,0:T(4,128)} %param.13) | copy-start | bytes 9220
  70.8 94.8 %copy-start.26 = (f32[3,256]{1,0:T(4,128)S(1)}, f32[3,256]{1,0:T(4,128)}, u32[]{:S(2)}) copy-start(f32[3,256]{1,0:T(4,128)} %param.14) | copy-start | bytes 9220
  70.8 94.8 %copy-start.22 = (f32[3,31,256]{2,1,0:T(8,128)S(1)}, f32[3,31,256]{2,1,0:T(8,128)}, u32[]{:S(2)}) copy-start(f32[3,31,256]{2,1,0:T(8,128)} %param.12) | copy-start | bytes 285700
  71.0 127.2 %copy-start.1 = (bf16[4,8,96,256]{3,2,1,0:T(8,128)(2,1)}, bf16[4,8,96,256]{3,2,1,0:T(8,128)(2,1)S(1)}, u32[]{:S(2)}) copy-start(bf16[4,8,96,256]{3,2,1,0:T(8,128)(2,1)S(1)} %pad_maximum_fusion.1.refs_12_) | copy-start | bytes 4718596
  71.0 100.4 %copy-start.24 = (f32[3,2048]{1,0:T(4,128)S(1)}, f32[3,2048]{1,0:T(4,128)}, u32[]{:S(2)}) copy-start(f32[3,2048]{1,0:T(4,128)} %param.9) | copy-start | bytes 73732
  71.1 101.6 %copy-start.23 = (bf16[96,512]{1,0:T(8,128)(2,1)}, bf16[96,512]{1,0:T(8,128)(2,1)S(1)}, u32[]{:S(2)}) copy-start(bf16[96,512]{1,0:T(8,128)(2,1)S(1)} %collective-permute-done.before_ref) | copy-start | bytes 294916
  71.1 18.9 %collective-permute-start.23 = (bf16[4,8,96,256]{3,2,1,0:T(8,128)(2,1)S(1)}, bf16[4,8,96,256]{3,2,1,0:T(8,128)(2,1)S(1)}, u32[]{:S(2)}, u32[]{:S(2)}) collective-permute-start(bf16[4,8,96,256]{3,2,1,0:T(8,128)(2,1)S(1)} %pad_maximum_fusion.refs_4_), channel_id=1, source_target_pairs={{0,4},{4,0},{1,5},{5,1},{2,6},{6,2},{3,7},{7,3},{8,12},{12,8},{9,1... | collective-permute-start | bytes 4718600 | tf_op jit(solution)/shard_map/ppermute | solution.py:308
  71.2 92.8 %copy-start.8 = (bf16[4,4,96,256]{3,2,1,0:T(8,128)(2,1)}, bf16[4,4,96,256]{3,2,1,0:T(8,128)(2,1)S(1)}, u32[]{:S(2)}) copy-start(bf16[4,4,96,256]{3,2,1,0:T(8,128)(2,1)S(1)} %collective-permute-done.4.refs_5_) | copy-start | bytes 2359300
  71.2 20.6 %collective-permute-start.35 = (bf16[4,8,96,256]{3,2,1,0:T(8,128)(2,1)S(1)}, bf16[4,8,96,256]{3,2,1,0:T(8,128)(2,1)}, u32[]{:S(2)}, u32[]{:S(2)}) collective-permute-start(bf16[4,8,96,256]{3,2,1,0:T(8,128)(2,1)S(1)} %pad_maximum_fusion.1.refs_12_), channel_id=1, source_target_pairs={{0,8},{4,28},{8,16},{12,4},{16,24},{20,12},{24,0},{28,20},{1,9},{5... | collective-permute-start | bytes 4718600 | tf_op jit(solution)/shard_map/ppermute | solution.py:318
  73.3 90.7 %copy-start.9 = (bf16[4,4,96,256]{3,2,1,0:T(8,128)(2,1)}, bf16[4,4,96,256]{3,2,1,0:T(8,128)(2,1)S(1)}, u32[]{:S(2)}) copy-start(bf16[4,4,96,256]{3,2,1,0:T(8,128)(2,1)S(1)} %collective-permute-done.9.refs_10_) | copy-start | bytes 2359300
  73.3 14.6 %collective-permute-start.6 = (bf16[4,4,96,256]{3,2,1,0:T(8,128)(2,1)S(1)}, bf16[4,4,96,256]{3,2,1,0:T(8,128)(2,1)S(1)}, u32[]{:S(2)}, u32[]{:S(2)}) collective-permute-start(bf16[4,4,96,256]{3,2,1,0:T(8,128)(2,1)S(1)} %collective-permute-done.4.refs_5_), channel_id=1, source_target_pairs={{0,32},{4,228},{32,64},{36,4},{64,96},{68,36},{96,128},{100,68},{1... | collective-permute-start | bytes 2359304 | tf_op jit(solution)/shard_map/ppermute | solution.py:318
  73.9 90.7 %copy-start.10 = (bf16[4,4,96,256]{3,2,1,0:T(8,128)(2,1)}, bf16[4,4,96,256]{3,2,1,0:T(8,128)(2,1)S(1)}, u32[]{:S(2)}) copy-start(bf16[4,4,96,256]{3,2,1,0:T(8,128)(2,1)S(1)} %collective-permute-done.7.refs_8_) | copy-start | bytes 2359300
  73.9 27.2 %collective-permute-start.34 = (bf16[4,8,96,256]{3,2,1,0:T(8,128)(2,1)S(1)}, bf16[4,8,96,256]{3,2,1,0:T(8,128)(2,1)S(1)}, u32[]{:S(2)}, u32[]{:S(2)}) collective-permute-start(bf16[4,8,96,256]{3,2,1,0:T(8,128)(2,1)S(1)} %pad_maximum_fusion.1.refs_12_), channel_id=1, source_target_pairs={{0,4},{4,0},{1,5},{5,1},{2,6},{6,2},{3,7},{7,3},{8,12},{12,8},{9,1... | collective-permute-start | bytes 4718600 | tf_op jit(solution)/shard_map/ppermute | solution.py:308
  87.9 76.7 %copy-start.11 = (bf16[4,4,96,256]{3,2,1,0:T(8,128)(2,1)}, bf16[4,4,96,256]{3,2,1,0:T(8,128)(2,1)S(1)}, u32[]{:S(2)}) copy-start(bf16[4,4,96,256]{3,2,1,0:T(8,128)(2,1)S(1)} %collective-permute-done.6.refs_7_) | copy-start | bytes 2359300
  87.9 13.2 %collective-permute-start.13 = (bf16[4,4,96,256]{3,2,1,0:T(8,128)(2,1)S(1)}, bf16[4,4,96,256]{3,2,1,0:T(8,128)(2,1)S(1)}, u32[]{:S(2)}, u32[]{:S(2)}) collective-permute-start(bf16[4,4,96,256]{3,2,1,0:T(8,128)(2,1)S(1)} %collective-permute-done.9.refs_10_), channel_id=1, source_target_pairs={{0,32},{4,228},{32,64},{36,4},{64,96},{68,36},{96,128},{100,68},{1... | collective-permute-start | bytes 2359304 | tf_op jit(solution)/shard_map/ppermute | solution.py:318
  90.0 28.0 %copy-start.3 = (bf16[4,8,96,256]{3,2,1,0:T(8,128)(2,1)}, bf16[4,8,96,256]{3,2,1,0:T(8,128)(2,1)S(1)}, u32[]{:S(2)}) copy-start(bf16[4,8,96,256]{3,2,1,0:T(8,128)(2,1)S(1)} %collective-permute-done.24.refs_6_) | copy-start | bytes 4718596
  90.0 19.6 %collective-permute-start.10 = (bf16[4,4,96,256]{3,2,1,0:T(8,128)(2,1)S(1)}, bf16[4,4,96,256]{3,2,1,0:T(8,128)(2,1)S(1)}, u32[]{:S(2)}, u32[]{:S(2)}) collective-permute-start(bf16[4,4,96,256]{3,2,1,0:T(8,128)(2,1)S(1)} %collective-permute-done.6.refs_7_), channel_id=1, source_target_pairs={{0,32},{4,228},{32,64},{36,4},{64,96},{68,36},{96,128},{100,68},{1... | collective-permute-start | bytes 2359304 | tf_op jit(solution)/shard_map/ppermute | solution.py:318
  90.0 42.0 %copy-start.4 = (bf16[4,8,96,256]{3,2,1,0:T(8,128)(2,1)}, bf16[4,8,96,256]{3,2,1,0:T(8,128)(2,1)S(1)}, u32[]{:S(2)}) copy-start(bf16[4,8,96,256]{3,2,1,0:T(8,128)(2,1)S(1)} %collective-permute-done.23.refs_5_) | copy-start | bytes 4718596
  90.0 19.6 %collective-permute-start.11 = (bf16[4,4,96,256]{3,2,1,0:T(8,128)(2,1)S(1)}, bf16[4,4,96,256]{3,2,1,0:T(8,128)(2,1)S(1)}, u32[]{:S(2)}, u32[]{:S(2)}) collective-permute-start(bf16[4,4,96,256]{3,2,1,0:T(8,128)(2,1)S(1)} %collective-permute-done.9.refs_10_), channel_id=1, source_target_pairs={{0,4},{4,0},{1,5},{5,1},{2,6},{6,2},{3,7},{7,3},{8,12},{12,8},{9,1... | collective-permute-start | bytes 2359304 | tf_op jit(solution)/shard_map/ppermute | solution.py:308
  91.8 17.9 %collective-permute-start.8 = (bf16[4,4,96,256]{3,2,1,0:T(8,128)(2,1)S(1)}, bf16[4,4,96,256]{3,2,1,0:T(8,128)(2,1)S(1)}, u32[]{:S(2)}, u32[]{:S(2)}) collective-permute-start(bf16[4,4,96,256]{3,2,1,0:T(8,128)(2,1)S(1)} %collective-permute-done.6.refs_7_), channel_id=1, source_target_pairs={{0,4},{4,0},{1,5},{5,1},{2,6},{6,2},{3,7},{7,3},{8,12},{12,8},{9,1... | collective-permute-start | bytes 2359304 | tf_op jit(solution)/shard_map/ppermute | solution.py:308
  101.1 97.1 %copy-start.12 = (bf16[4,4,96,256]{3,2,1,0:T(8,128)(2,1)}, bf16[4,4,96,256]{3,2,1,0:T(8,128)(2,1)S(1)}, u32[]{:S(2)}) copy-start(bf16[4,4,96,256]{3,2,1,0:T(8,128)(2,1)S(1)} %collective-permute-done.13.refs_14_) | copy-start | bytes 2359300
  101.1 16.9 %collective-permute-start.17 = (bf16[4,4,96,256]{3,2,1,0:T(8,128)(2,1)S(1)}, bf16[4,4,96,256]{3,2,1,0:T(8,128)(2,1)S(1)}, u32[]{:S(2)}, u32[]{:S(2)}) collective-permute-start(bf16[4,4,96,256]{3,2,1,0:T(8,128)(2,1)S(1)} %collective-permute-done.13.refs_14_), channel_id=1, source_target_pairs={{0,32},{4,228},{32,64},{36,4},{64,96},{68,36},{96,128},{100,68},{1... | collective-permute-start | bytes 2359304 | tf_op jit(solution)/shard_map/ppermute | solution.py:318
  101.1 47.7 %copy-start.5 = (bf16[4,8,96,256]{3,2,1,0:T(8,128)(2,1)}, bf16[4,8,96,256]{3,2,1,0:T(8,128)(2,1)S(1)}, u32[]{:S(2)}) copy-start(bf16[4,8,96,256]{3,2,1,0:T(8,128)(2,1)S(1)} %collective-permute-done.34.refs_13_) | copy-start | bytes 4718596
  101.1 16.8 %collective-permute-start.15 = (bf16[4,4,96,256]{3,2,1,0:T(8,128)(2,1)S(1)}, bf16[4,4,96,256]{3,2,1,0:T(8,128)(2,1)S(1)}, u32[]{:S(2)}, u32[]{:S(2)}) collective-permute-start(bf16[4,4,96,256]{3,2,1,0:T(8,128)(2,1)S(1)} %collective-permute-done.13.refs_14_), channel_id=1, source_target_pairs={{0,4},{4,0},{1,5},{5,1},{2,6},{6,2},{3,7},{7,3},{8,12},{12,8},{9,1... | collective-permute-start | bytes 2359304 | tf_op jit(solution)/shard_map/ppermute | solution.py:308
  109.5 55.2 %copy-start.13 = (bf16[4,4,96,256]{3,2,1,0:T(8,128)(2,1)}, bf16[4,4,96,256]{3,2,1,0:T(8,128)(2,1)S(1)}, u32[]{:S(2)}) copy-start(bf16[4,4,96,256]{3,2,1,0:T(8,128)(2,1)S(1)} %collective-permute-done.10.refs_11_) | copy-start | bytes 2359300
  109.5 16.9 %collective-permute-start.14 = (bf16[4,4,96,256]{3,2,1,0:T(8,128)(2,1)S(1)}, bf16[4,4,96,256]{3,2,1,0:T(8,128)(2,1)S(1)}, u32[]{:S(2)}, u32[]{:S(2)}) collective-permute-start(bf16[4,4,96,256]{3,2,1,0:T(8,128)(2,1)S(1)} %collective-permute-done.10.refs_11_), channel_id=1, source_target_pairs={{0,32},{4,228},{32,64},{36,4},{64,96},{68,36},{96,128},{100,68},{1... | collective-permute-start | bytes 2359304 | tf_op jit(solution)/shard_map/ppermute | solution.py:318
  109.6 16.9 %collective-permute-start.12 = (bf16[4,4,96,256]{3,2,1,0:T(8,128)(2,1)S(1)}, bf16[4,4,96,256]{3,2,1,0:T(8,128)(2,1)S(1)}, u32[]{:S(2)}, u32[]{:S(2)}) collective-permute-start(bf16[4,4,96,256]{3,2,1,0:T(8,128)(2,1)S(1)} %collective-permute-done.10.refs_11_), channel_id=1, source_target_pairs={{0,4},{4,0},{1,5},{5,1},{2,6},{6,2},{3,7},{7,3},{8,12},{12,8},{9,1... | collective-permute-start | bytes 2359304 | tf_op jit(solution)/shard_map/ppermute | solution.py:308
  109.7 22.3 %collective-permute-start.28 = (bf16[4,8,96,256]{3,2,1,0:T(8,128)(2,1)S(1)}, bf16[4,8,96,256]{3,2,1,0:T(8,128)(2,1)}, u32[]{:S(2)}, u32[]{:S(2)}) collective-permute-start(bf16[4,8,96,256]{3,2,1,0:T(8,128)(2,1)S(1)} %collective-permute-done.24.refs_6_), channel_id=1, source_target_pairs={{0,1},{4,7},{1,2},{5,4},{2,3},{6,5},{3,0},{7,6},{8,9},{12,15},{9,1... | collective-permute-start | bytes 4718600 | tf_op jit(solution)/shard_map/ppermute | solution.py:318
  118.0 46.8 %copy-start.16 = (bf16[4,4,96,256]{3,2,1,0:T(8,128)(2,1)}, bf16[4,4,96,256]{3,2,1,0:T(8,128)(2,1)S(1)}, u32[]{:S(2)}) copy-start(bf16[4,4,96,256]{3,2,1,0:T(8,128)(2,1)S(1)} %collective-permute-done.17.refs_18_) | copy-start | bytes 2359300
  118.0 14.0 %collective-permute-start.26 = (bf16[4,8,96,256]{3,2,1,0:T(8,128)(2,1)S(1)}, bf16[4,8,96,256]{3,2,1,0:T(8,128)(2,1)S(1)}, u32[]{:S(2)}, u32[]{:S(2)}) collective-permute-start(bf16[4,8,96,256]{3,2,1,0:T(8,128)(2,1)S(1)} %collective-permute-done.24.refs_6_), channel_id=1, source_target_pairs={{0,4},{4,0},{1,5},{5,1},{2,6},{6,2},{3,7},{7,3},{8,12},{12,8},{9,1... | collective-permute-start | bytes 4718600 | tf_op jit(solution)/shard_map/ppermute | solution.py:308
  118.0 46.8 %copy-start.17 = (bf16[4,4,96,256]{3,2,1,0:T(8,128)(2,1)}, bf16[4,4,96,256]{3,2,1,0:T(8,128)(2,1)S(1)}, u32[]{:S(2)}) copy-start(bf16[4,4,96,256]{3,2,1,0:T(8,128)(2,1)S(1)} %collective-permute-done.15.refs_16_) | copy-start | bytes 2359300
  118.0 30.8 %collective-permute-start.25 = (bf16[4,8,96,256]{3,2,1,0:T(8,128)(2,1)S(1)}, bf16[4,8,96,256]{3,2,1,0:T(8,128)(2,1)}, u32[]{:S(2)}, u32[]{:S(2)}) collective-permute-start(bf16[4,8,96,256]{3,2,1,0:T(8,128)(2,1)S(1)} %collective-permute-done.23.refs_5_), channel_id=1, source_target_pairs={{0,1},{4,7},{1,2},{5,4},{2,3},{6,5},{3,0},{7,6},{8,9},{12,15},{9,1... | collective-permute-start | bytes 4718600 | tf_op jit(solution)/shard_map/ppermute | solution.py:318
  126.4 38.4 %copy-start.18 = (bf16[4,4,96,256]{3,2,1,0:T(8,128)(2,1)}, bf16[4,4,96,256]{3,2,1,0:T(8,128)(2,1)S(1)}, u32[]{:S(2)}) copy-start(bf16[4,4,96,256]{3,2,1,0:T(8,128)(2,1)S(1)} %collective-permute-done.14.refs_15_) | copy-start | bytes 2359300
  126.4 22.4 %collective-permute-start.39 = (bf16[4,8,96,256]{3,2,1,0:T(8,128)(2,1)}, bf16[4,8,96,256]{3,2,1,0:T(8,128)(2,1)}, u32[]{:S(2)}, u32[]{:S(2)}) collective-permute-start(bf16[4,8,96,256]{3,2,1,0:T(8,128)(2,1)} %collective-permute-done.35.refs_14_), channel_id=1, source_target_pairs={{0,8},{4,28},{8,16},{12,4},{16,24},{20,12},{24,0},{28,20},{1,9},{5... | collective-permute-start | bytes 4718600 | tf_op jit(solution)/shard_map/ppermute | solution.py:318
  126.5 38.3 %copy-start.19 = (bf16[4,4,96,256]{3,2,1,0:T(8,128)(2,1)}, bf16[4,4,96,256]{3,2,1,0:T(8,128)(2,1)S(1)}, u32[]{:S(2)}) copy-start(bf16[4,4,96,256]{3,2,1,0:T(8,128)(2,1)S(1)} %collective-permute-done.12.refs_13_) | copy-start | bytes 2359300
  126.5 37.5 %collective-permute-start.36 = (bf16[4,8,96,256]{3,2,1,0:T(8,128)(2,1)S(1)}, bf16[4,8,96,256]{3,2,1,0:T(8,128)(2,1)}, u32[]{:S(2)}, u32[]{:S(2)}) collective-permute-start(bf16[4,8,96,256]{3,2,1,0:T(8,128)(2,1)S(1)} %collective-permute-done.34.refs_13_), channel_id=1, source_target_pairs={{0,8},{4,28},{8,16},{12,4},{16,24},{20,12},{24,0},{28,20},{1,9},{5... | collective-permute-start | bytes 4718600 | tf_op jit(solution)/shard_map/ppermute | solution.py:318
  132.0 32.0 %collective-permute-start.18 = (bf16[4,4,96,256]{3,2,1,0:T(8,128)(2,1)S(1)}, bf16[4,4,96,256]{3,2,1,0:T(8,128)(2,1)S(1)}, u32[]{:S(2)}, u32[]{:S(2)}) collective-permute-start(bf16[4,4,96,256]{3,2,1,0:T(8,128)(2,1)S(1)} %collective-permute-done.17.refs_18_), channel_id=1, source_target_pairs={{0,4},{4,0},{1,5},{5,1},{2,6},{6,2},{3,7},{7,3},{8,12},{12,8},{9,1... | collective-permute-start | bytes 2359304 | tf_op jit(solution)/shard_map/ppermute | solution.py:308
  132.0 32.0 %copy-start.6 = (bf16[4,8,96,256]{3,2,1,0:T(8,128)(2,1)}, bf16[4,8,96,256]{3,2,1,0:T(8,128)(2,1)S(1)}, u32[]{:S(2)}) copy-start(bf16[4,8,96,256]{3,2,1,0:T(8,128)(2,1)S(1)} %collective-permute-done.26.refs_8_) | copy-start | bytes 4718596
  132.0 32.6 %collective-permute-start.16 = (bf16[4,4,96,256]{3,2,1,0:T(8,128)(2,1)S(1)}, bf16[4,4,96,256]{3,2,1,0:T(8,128)(2,1)S(1)}, u32[]{:S(2)}, u32[]{:S(2)}) collective-permute-start(bf16[4,4,96,256]{3,2,1,0:T(8,128)(2,1)S(1)} %collective-permute-done.14.refs_15_), channel_id=1, source_target_pairs={{0,4},{4,0},{1,5},{5,1},{2,6},{6,2},{3,7},{7,3},{8,12},{12,8},{9,1... | collective-permute-start | bytes 2359304 | tf_op jit(solution)/shard_map/ppermute | solution.py:308
  148.8 65.1 %collective-permute-start.37 = (bf16[4,8,96,256]{3,2,1,0:T(8,128)(2,1)}, bf16[4,8,96,256]{3,2,1,0:T(8,128)(2,1)}, u32[]{:S(2)}, u32[]{:S(2)}) collective-permute-start(bf16[4,8,96,256]{3,2,1,0:T(8,128)(2,1)} %collective-permute-done.35.refs_14_), channel_id=1, source_target_pairs={{0,4},{4,0},{1,5},{5,1},{2,6},{6,2},{3,7},{7,3},{8,12},{12,8},{9,1... | collective-permute-start | bytes 4718600 | tf_op jit(solution)/shard_map/ppermute | solution.py:308
  148.8 65.1 %collective-permute-start.29 = (bf16[4,8,96,256]{3,2,1,0:T(8,128)(2,1)}, bf16[4,8,96,256]{3,2,1,0:T(8,128)(2,1)}, u32[]{:S(2)}, u32[]{:S(2)}) collective-permute-start(bf16[4,8,96,256]{3,2,1,0:T(8,128)(2,1)} %collective-permute-done.28.refs_10_), channel_id=1, source_target_pairs={{0,4},{4,0},{1,5},{5,1},{2,6},{6,2},{3,7},{7,3},{8,12},{12,8},{9,1... | collective-permute-start | bytes 4718600 | tf_op jit(solution)/shard_map/ppermute | solution.py:308
  164.0 49.9 %collective-permute-start.27 = (bf16[4,8,96,256]{3,2,1,0:T(8,128)(2,1)}, bf16[4,8,96,256]{3,2,1,0:T(8,128)(2,1)}, u32[]{:S(2)}, u32[]{:S(2)}) collective-permute-start(bf16[4,8,96,256]{3,2,1,0:T(8,128)(2,1)} %collective-permute-done.25.refs_7_), channel_id=1, source_target_pairs={{0,4},{4,0},{1,5},{5,1},{2,6},{6,2},{3,7},{7,3},{8,12},{12,8},{9,1... | collective-permute-start | bytes 4718600 | tf_op jit(solution)/shard_map/ppermute | solution.py:308
  164.0 49.9 %collective-permute-start.40 = (bf16[4,8,96,256]{3,2,1,0:T(8,128)(2,1)}, bf16[4,8,96,256]{3,2,1,0:T(8,128)(2,1)}, u32[]{:S(2)}, u32[]{:S(2)}) collective-permute-start(bf16[4,8,96,256]{3,2,1,0:T(8,128)(2,1)} %collective-permute-done.39.refs_18_), channel_id=1, source_target_pairs={{0,4},{4,0},{1,5},{5,1},{2,6},{6,2},{3,7},{7,3},{8,12},{12,8},{9,1... | collective-permute-start | bytes 4718600 | tf_op jit(solution)/shard_map/ppermute | solution.py:308
  164.6 49.3 %collective-permute-start.38 = (bf16[4,8,96,256]{3,2,1,0:T(8,128)(2,1)}, bf16[4,8,96,256]{3,2,1,0:T(8,128)(2,1)}, u32[]{:S(2)}, u32[]{:S(2)}) collective-permute-start(bf16[4,8,96,256]{3,2,1,0:T(8,128)(2,1)} %collective-permute-done.36.refs_15_), channel_id=1, source_target_pairs={{0,4},{4,0},{1,5},{5,1},{2,6},{6,2},{3,7},{7,3},{8,12},{12,8},{9,1... | collective-permute-start | bytes 4718600 | tf_op jit(solution)/shard_map/ppermute | solution.py:308
  166.4 14.4 %all-to-all-start.1 = ((f32[4,3,33,256]{3,2,1,0:T(8,128)}), f32[4,3,33,256]{3,2,1,0:T(8,128)S(1)}, u32[]{:S(2)}, u32[]{:S(2)}) async-start(f32[4,3,33,256]{3,2,1,0:T(8,128)} %broadcast_in_dim.17), calls=%async_computation.1 | async-start | bytes 983040 | tf_op jit(solution)/shard_map/all_to_all | solution.py:285
  (7 other events, 42.1 us)

commit v2 on v1

--- a/solution.py
+++ b/solution.py
@@ -10,7 +10,7 @@
 
 NZ, NX, NC, NY = 8, 4, 2, 4
 HALO = 32
-ROWS = 32
+ROWS = 64
 TILE = 8
 DEPTH, WIDE = 32, 256
 GROUP = NX * NC * DEPTH
@@ -105,6 +105,7 @@
     lax.fori_loop(0, NZ, normalised, 0)
 
     lead = HALO - reach
+    count = max(c for c in range(TILE, ROWS + 1, TILE) if rows % c == 0)
     row = lax.broadcasted_iota(jnp.int32, (rows_in, 1), 0)
     ahead = row < info_ref[4 + layer]
 
@@ -125,20 +126,20 @@
         glu_ref[:rows_in] = jnp.where(ahead, 0.0, glu)
 
         def filtered(i, carry):
-            r = pl.multiple_of(i * ROWS, ROWS)
-            acc = jnp.zeros((ROWS, WIDE), jnp.float32)
+            r = pl.multiple_of(i * count, count)
+            acc = jnp.zeros((count, WIDE), jnp.float32)
             for s in range(TILE):
                 extra = TILE if s else 0
-                part = jnp.zeros((ROWS + extra, WIDE), jnp.float32)
+                part = jnp.zeros((count + extra, WIDE), jnp.float32)
                 for tap in range(reach + 1):
                     if (tap + lead) % TILE == s:
                         at = pl.multiple_of(r + (tap + lead - s), TILE)
-                        part = part + small_of(dy, layer, tap) * glu_ref[pl.ds(at, ROWS + extra), :]
-                acc = acc + part[s : s + ROWS]
-            fil_ref[dy, pl.ds(r, ROWS), :] = acc
+                        part = part + small_of(dy, layer, tap) * glu_ref[pl.ds(at, count + extra), :]
+                acc = acc + part[s : s + count]
+            fil_ref[dy, pl.ds(r, count), :] = acc
             return carry
 
-        lax.fori_loop(0, rows // ROWS, filtered, 0)
+        lax.fori_loop(0, rows // count, filtered, 0)
         return carry
 
     lax.fori_loop(0, NY, block, 0)

time: 249 us -> 248 us (level)
  no operation moved by 1% of the time
where the time goes in v2:
time: 248 us
  waiting for transfers between devices  116 us (47%)
  starting transfers between devices  48.9 us (20%)
  Pallas kernels  43.7 us (18%)
  blocking collectives  28.9 us (12%)
  local copies, waits for them, and re-layouts  6.66 us (3%)
  other arithmetic  3.46 us (1%)
    ppermute x13, waiting for transfers between devices, sent(): return lax.ppermute(a, axes, route)  87 us
    pallas_call x2, Pallas kernels, modules(): pl.pallas_call(functools.partial(modules_kernel, first, [len(p) for p in...  37 us
    all_to_all x3, starting transfers between devices, to_each(): lax.all_to_all(jnp.broadcast_to(a, (SPAN[axis], *a.shape)), axis, 0, 0, t...  18.2 us
    all_to_all x1, blocking collectives, shards(): lax.all_to_all(windows, 'y', 0, 0, tiled=True)  17.4 us
    ppermute x11, waiting for transfers between devices, shift(): return lax.ppermute(a, axis, [(i, (i + by) % n) for i in range(n)])  17.1 us
    ppermute x11, starting transfers between devices, shift(): return lax.ppermute(a, axis, [(i, (i + by) % n) for i in range(n)])  16.9 us
    all_to_all x1, blocking collectives, shards(): return lax.all_to_all(x, 'y', 0, 0, tiled=True).reshape(inputs.shape)  11.5 us
    all_to_all x3, waiting for transfers between devices, to_each(): lax.all_to_all(jnp.broadcast_to(a, (SPAN[axis], *a.shape)), axis, 0, 0, t...  11.3 us
  transfers between devices with their start and end apart: 44, of which 22 were waited for; matrix products, arithmetic and copies ran while one was open for 2% of the time, Pallas kernels for 9%

profile of v2, /device:TPU:4, one launch (start us, length us, event | category | flops | bytes accessed | tf_op | source)
XLA Modules:
  0.0 247.6 jit_solution(269124153848459575)
XLA Ops:
  0.0 0.8 maximum_bitcast_fusion.2
  0.8 0.7 broadcast_in_dim.18
  1.4 5.5 %all-to-all-start.2 = ((bf16[4,96,256]{2,1,0:T(8,128)(2,1)}), bf16[4,96,256]{2,1,0:T(8,128)(2,1)S(1)}, u32[]{:S(2)}, u32[]{:S(2)}) async-start(bf16[4,96,256]{2,1,0:T(8,128)(2,1)} %broadcast_in_dim.18), calls=%async_computation.2 | async-start | bytes 393216 | tf_op jit(solution)/shard_map/all_to_all | solution.py:286
  7.0 0.8 pad_maximum_fusion.4
  7.8 2.6 %all-to-all-done.2 = bf16[4,96,256]{2,1,0:T(8,128)(2,1)S(1)} async-done(((bf16[4,96,256]{2,1,0:T(8,128)(2,1)}), bf16[4,96,256]{2,1,0:T(8,128)(2,1)S(1)}, u32[]{:S(2)}, u32[]{:S(2)}) %all-to-all-start.2) | async-done | bytes 196640 | tf_op jit(solution)/shard_map/all_to_all | solution.py:286
  10.4 1.0 broadcast_in_dim.19
  11.4 7.7 %all-to-all-start.3 = ((bf16[8,2,96,256]{3,2,1,0:T(8,128)(2,1)}), bf16[8,2,96,256]{3,2,1,0:T(8,128)(2,1)S(1)}, u32[]{:S(2)}, u32[]{:S(2)}) async-start(bf16[8,2,96,256]{3,2,1,0:T(8,128)(2,1)} %broadcast_in_dim.19), calls=%async_computation.3 | async-start | bytes 1572864 | tf_op jit(solution)/shard_map/all_to_all | solution.py:286
  19.2 3.1 %collective-permute-start.1 = (bf16[4,96,256]{2,1,0:T(8,128)(2,1)S(1)}, bf16[4,96,256]{2,1,0:T(8,128)(2,1)S(1)}, u32[]{:S(2)}, u32[]{:S(2)}) collective-permute-start(bf16[4,96,256]{2,1,0:T(8,128)(2,1)S(1)} %fusion.1), channel_id=1, source_target_pairs={{0,3},{1,0},{2,1},{3,2},{4,7},{5,4},{6,5},{7,6},{8,11},{9,8},{10,9... | collective-permute-start | bytes 589832 | tf_op jit(solution)/shard_map/ppermute | solution.py:282
  22.3 0.6 collective-permute-start.2
  23.0 1.0 collective-permute-start.3
  24.0 5.0 %collective-permute-done.1 = bf16[4,96,256]{2,1,0:T(8,128)(2,1)S(1)} collective-permute-done((bf16[4,96,256]{2,1,0:T(8,128)(2,1)S(1)}, bf16[4,96,256]{2,1,0:T(8,128)(2,1)S(1)}, u32[]{:S(2)}, u32[]{:S(2)}) %collective-permute-start.1) | collective-permute-done | bytes 196640 | tf_op jit(solution)/shard_map/ppermute | solution.py:282
  29.0 1.6 collective-permute-done.2
  30.6 2.1 collective-permute-done.3
  32.7 1.0 pad_maximum_fusion.2.refs_4_
  33.7 7.2 %all-to-all-done.3 = bf16[8,2,96,256]{3,2,1,0:T(8,128)(2,1)S(1)} async-done(((bf16[8,2,96,256]{3,2,1,0:T(8,128)(2,1)}), bf16[8,2,96,256]{3,2,1,0:T(8,128)(2,1)S(1)}, u32[]{:S(2)}, u32[]{:S(2)}) %all-to-all-start.3) | async-done | bytes 786464 | tf_op jit(solution)/shard_map/all_to_all | solution.py:286
  40.8 0.7 collective-permute-start.5
  42.0 2.1 collective-permute-start.20
  44.2 1.6 collective-permute-start.31
  45.7 1.7 collective-permute-start.30
  47.4 3.4 %collective-permute-done.20 = bf16[8,96,256]{2,1,0:T(8,128)(2,1)S(1)} collective-permute-done((bf16[8,96,256]{2,1,0:T(8,128)(2,1)S(1)}, bf16[8,96,256]{2,1,0:T(8,128)(2,1)S(1)}, u32[]{:S(2)}, u32[]{:S(2)}) %collective-permute-start.20) | collective-permute-done | bytes 393248 | tf_op jit(solution)/shard_map/ppermute | solution.py:282
  50.8 3.5 %collective-permute-done.5.refs_6_ = bf16[4,4,96,256]{3,2,1,0:T(8,128)(2,1)S(1)} collective-permute-done((bf16[4,4,96,256]{3,2,1,0:T(8,128)(2,1)}, bf16[4,4,96,256]{3,2,1,0:T(8,128)(2,1)S(1)}, u32[]{:S(2)}, u32[]{:S(2)}) %collective-permute-start.5) | collective-permute-done | bytes 786464 | tf_op jit(solution)/shard_map/ppermute | solution.py:319
  54.3 2.1 collective-permute-start.21
  56.5 0.9 slice.27
  57.4 1.9 collective-permute-start
  59.4 0.7 collective-permute-done.21
  60.0 1.6 collective-permute-start.32
  61.6 1.3 collective-permute-done.22
  62.9 3.0 %collective-permute-start.33 = (bf16[4,96,256]{2,1,0:T(8,128)(2,1)S(1)}, bf16[4,96,256]{2,1,0:T(8,128)(2,1)S(1)}, u32[]{:S(2)}, u32[]{:S(2)}) collective-permute-start(bf16[4,96,256]{2,1,0:T(8,128)(2,1)S(1)} %slice.41), channel_id=1, source_target_pairs={{0,3},{1,0},{2,1},{3,2},{4,7},{5,4},{6,5},{7,6},{8,11},{9,8},{10,9... | collective-permute-start | bytes 589832 | tf_op jit(solution)/shard_map/ppermute | solution.py:282
  66.2 2.2 collective-permute-done.32
  68.3 0.4 collective-permute-start.24
  68.8 0.9 collective-permute-done.33
  69.8 1.0 collective-permute-start.7
  71.2 2.1 collective-permute-start.35
  73.3 0.6 collective-permute-start.6
  73.9 0.8 collective-permute-start.34
  74.7 13.2 %collective-permute-done.6.refs_7_ = bf16[4,4,96,256]{3,2,1,0:T(8,128)(2,1)S(1)} collective-permute-done((bf16[4,4,96,256]{3,2,1,0:T(8,128)(2,1)S(1)}, bf16[4,4,96,256]{3,2,1,0:T(8,128)(2,1)S(1)}, u32[]{:S(2)}, u32[]{:S(2)}) %collective-permute-start.6) | collective-permute-done | bytes 786464 | tf_op jit(solution)/shard_map/ppermute | solution.py:319
  87.9 2.1 collective-permute-done.24.refs_6_
  90.0 1.5 collective-permute-start.11
  91.5 0.3 collective-permute-done.35.refs_14_
  91.8 9.3 %collective-permute-done.13.refs_14_ = bf16[4,4,96,256]{3,2,1,0:T(8,128)(2,1)S(1)} collective-permute-done((bf16[4,4,96,256]{3,2,1,0:T(8,128)(2,1)S(1)}, bf16[4,4,96,256]{3,2,1,0:T(8,128)(2,1)S(1)}, u32[]{:S(2)}, u32[]{:S(2)}) %collective-permute-start.13) | collective-permute-done | bytes 786464 | tf_op jit(solution)/shard_map/ppermute | solution.py:319
  101.2 8.3 %collective-permute-done.10.refs_11_ = bf16[4,4,96,256]{3,2,1,0:T(8,128)(2,1)S(1)} collective-permute-done((bf16[4,4,96,256]{3,2,1,0:T(8,128)(2,1)S(1)}, bf16[4,4,96,256]{3,2,1,0:T(8,128)(2,1)S(1)}, u32[]{:S(2)}, u32[]{:S(2)}) %collective-permute-start.10) | collective-permute-done | bytes 786464 | tf_op jit(solution)/shard_map/ppermute | solution.py:319
  109.7 1.1 collective-permute-start.28
  110.9 7.0 %collective-permute-done.17.refs_18_ = bf16[4,4,96,256]{3,2,1,0:T(8,128)(2,1)S(1)} collective-permute-done((bf16[4,4,96,256]{3,2,1,0:T(8,128)(2,1)S(1)}, bf16[4,4,96,256]{3,2,1,0:T(8,128)(2,1)S(1)}, u32[]{:S(2)}, u32[]{:S(2)}) %collective-permute-start.17) | collective-permute-done | bytes 786464 | tf_op jit(solution)/shard_map/ppermute | solution.py:319
  118.0 1.1 collective-permute-start.25
  119.1 7.3 %collective-permute-done.14.refs_15_ = bf16[4,4,96,256]{3,2,1,0:T(8,128)(2,1)S(1)} collective-permute-done((bf16[4,4,96,256]{3,2,1,0:T(8,128)(2,1)S(1)}, bf16[4,4,96,256]{3,2,1,0:T(8,128)(2,1)S(1)}, u32[]{:S(2)}, u32[]{:S(2)}) %collective-permute-start.14) | collective-permute-done | bytes 786464 | tf_op jit(solution)/shard_map/ppermute | solution.py:319
  126.5 0.3 collective-permute-start.36
  126.8 5.1 %collective-permute-done.28.refs_10_ = bf16[4,8,96,256]{3,2,1,0:T(8,128)(2,1)} collective-permute-done((bf16[4,8,96,256]{3,2,1,0:T(8,128)(2,1)S(1)}, bf16[4,8,96,256]{3,2,1,0:T(8,128)(2,1)}, u32[]{:S(2)}, u32[]{:S(2)}) %collective-permute-start.28) | collective-permute-done | bytes 1572896 | tf_op jit(solution)/shard_map/ppermute | solution.py:319
  132.0 0.6 collective-permute-start.16
  132.6 16.3 %collective-permute-done.25.refs_7_ = bf16[4,8,96,256]{3,2,1,0:T(8,128)(2,1)} collective-permute-done((bf16[4,8,96,256]{3,2,1,0:T(8,128)(2,1)S(1)}, bf16[4,8,96,256]{3,2,1,0:T(8,128)(2,1)}, u32[]{:S(2)}, u32[]{:S(2)}) %collective-permute-start.25) | collective-permute-done | bytes 1572896 | tf_op jit(solution)/shard_map/ppermute | solution.py:319
  148.8 0.5 collective-permute-start.29
  149.3 14.7 %collective-permute-done.36.refs_15_ = bf16[4,8,96,256]{3,2,1,0:T(8,128)(2,1)} collective-permute-done((bf16[4,8,96,256]{3,2,1,0:T(8,128)(2,1)S(1)}, bf16[4,8,96,256]{3,2,1,0:T(8,128)(2,1)}, u32[]{:S(2)}, u32[]{:S(2)}) %collective-permute-start.36) | collective-permute-done | bytes 1572896 | tf_op jit(solution)/shard_map/ppermute | solution.py:319
  164.0 0.6 collective-permute-start.40
  164.9 0.7 copy-done.21
  165.6 0.8 broadcast_in_dim.17
  166.4 5.0 %all-to-all-start.1 = ((f32[4,3,33,256]{3,2,1,0:T(8,128)}), f32[4,3,33,256]{3,2,1,0:T(8,128)S(1)}, u32[]{:S(2)}, u32[]{:S(2)}) async-start(f32[4,3,33,256]{3,2,1,0:T(8,128)} %broadcast_in_dim.17), calls=%async_computation.1 | async-start | bytes 983040 | tf_op jit(solution)/shard_map/all_to_all | solution.py:286
  171.4 0.6 copy.21
  172.0 0.6 stack.74.info_ref.refs_0_
  172.6 6.6 %prepare.1 = (bf16[4,2,224,256]{3,2,1,0:T(8,128)(2,1)}, f32[3,8,256]{2,1,0:T(8,128)}) custom-call(s32[8]{0:T(128)} %stack.74.info_ref.refs_0_, bf16[96,512]{1,0:T(8,128)(2,1)} %copy-done.23, bf16[512,512]{1,0:T(8,128)(2,1)} %x_ref.1, f32[3,8,256]{2,1,0:T(8,128)} %bitcast.57), custom_call_target="tpu_custom_call" | custom-call | tf_op jit(solution)/shard_map/prepare/pallas_call | solution.py:70
  179.3 1.5 all-to-all-done.1.refs_3_
  180.8 17.4 %all_to_all.25 = bf16[4,2,224,256]{3,2,1,0:T(8,128)(2,1)} all-to-all(bf16[4,2,224,256]{3,2,1,0:T(8,128)(2,1)} %get-tuple-element.9), channel_id=1, replica_groups=mesh['z'=8,'x'=4,'c'=2,'y'=4] {'y'}, dimensions={0} | all-to-all | bytes 1835008 | tf_op jit(solution)/shard_map/all_to_all | solution.py:342
  198.2 15.4 %shard_map.82.refs_1_ = bf16[8,192,256]{2,1,0:T(8,128)(2,1)} custom-call(s32[8]{0:T(128)} %stack.74.info_ref.refs_0_, bf16[8,224,256]{2,1,0:T(8,128)(2,1)} %bitcast.46, f32[3,8,256]{2,1,0:T(8,128)} %get-tuple-element.10.refs_2_, f32[4,3,33,256]{3,2,1,0:T(8,128)} %copy-done.2, bf16[4,4,96,256]{3,2,1,0:T(8,128)(2,1)} %pad_maximum_fusion.2.refs_4_, ...), custom_call_target="tpu_custom_call" | custom-call | flops 2818572288 | bytes 12582912 | tf_op jit(solution)/shard_map/pallas_call | solution.py:251
  213.6 21.6 %shard_map.83 = bf16[4,128,512]{2,1,0:T(8,128)(2,1)} custom-call(s32[8]{0:T(128)} %stack.74.info_ref.refs_0_, bf16[8,192,256]{2,1,0:T(8,128)(2,1)} %shard_map.82.refs_1_, f32[3,8,256]{2,1,0:T(8,128)} %get-tuple-element.10.refs_2_, f32[4,3,33,256]{3,2,1,0:T(8,128)} %copy-done.2, bf16[4,8,96,256]{3,2,1,0:T(8,128)(2,1)} %copy-done, ...), custom_call_target="tpu_custom_call" | custom-call | flops 4831838208 | bytes 25165824 | tf_op jit(solution)/shard_map/pallas_call | solution.py:251
  235.3 11.5 %all_to_all.26 = bf16[4,128,512]{2,1,0:T(8,128)(2,1)S(1)} all-to-all(bf16[4,128,512]{2,1,0:T(8,128)(2,1)} %shard_map.83), channel_id=1, replica_groups=mesh['z'=8,'x'=4,'c'=2,'y'=4] {'y'}, dimensions={0} | all-to-all | bytes 1048576 | tf_op jit(solution)/shard_map/all_to_all | solution.py:359
  246.8 0.8 copy.23
  (108 shorter events, 2.3 us)
Async XLA Ops:
  1.4 9.0 %all-to-all-start.2 = ((bf16[4,96,256]{2,1,0:T(8,128)(2,1)}), bf16[4,96,256]{2,1,0:T(8,128)(2,1)S(1)}, u32[]{:S(2)}, u32[]{:S(2)}) async-start(bf16[4,96,256]{2,1,0:T(8,128)(2,1)} %broadcast_in_dim.18), calls=%async_computation.2 | async-start | bytes 393216 | tf_op jit(solution)/shard_map/all_to_all | solution.py:286
  11.4 29.4 %all-to-all-start.3 = ((bf16[8,2,96,256]{3,2,1,0:T(8,128)(2,1)}), bf16[8,2,96,256]{3,2,1,0:T(8,128)(2,1)S(1)}, u32[]{:S(2)}, u32[]{:S(2)}) async-start(bf16[8,2,96,256]{3,2,1,0:T(8,128)(2,1)} %broadcast_in_dim.19), calls=%async_computation.3 | async-start | bytes 1572864 | tf_op jit(solution)/shard_map/all_to_all | solution.py:286
  19.2 9.8 %collective-permute-start.1 = (bf16[4,96,256]{2,1,0:T(8,128)(2,1)S(1)}, bf16[4,96,256]{2,1,0:T(8,128)(2,1)S(1)}, u32[]{:S(2)}, u32[]{:S(2)}) collective-permute-start(bf16[4,96,256]{2,1,0:T(8,128)(2,1)S(1)} %fusion.1), channel_id=1, source_target_pairs={{0,3},{1,0},{2,1},{3,2},{4,7},{5,4},{6,5},{7,6},{8,11},{9,8},{10,9... | collective-permute-start | bytes 589832 | tf_op jit(solution)/shard_map/ppermute | solution.py:282
  22.3 8.3 %collective-permute-start.2 = (bf16[4,96,256]{2,1,0:T(8,128)(2,1)S(1)}, bf16[4,96,256]{2,1,0:T(8,128)(2,1)S(1)}, u32[]{:S(2)}, u32[]{:S(2)}) collective-permute-start(bf16[4,96,256]{2,1,0:T(8,128)(2,1)S(1)} %fusion.1), channel_id=1, source_target_pairs={{0,2},{1,3},{2,0},{3,1},{4,6},{5,7},{6,4},{7,5},{8,10},{9,11},{10,... | collective-permute-start | bytes 589832 | tf_op jit(solution)/shard_map/ppermute | solution.py:282
  23.0 9.7 %collective-permute-start.3 = (bf16[4,96,256]{2,1,0:T(8,128)(2,1)S(1)}, bf16[4,96,256]{2,1,0:T(8,128)(2,1)S(1)}, u32[]{:S(2)}, u32[]{:S(2)}) collective-permute-start(bf16[4,96,256]{2,1,0:T(8,128)(2,1)S(1)} %fusion.1), channel_id=1, source_target_pairs={{0,1},{1,2},{2,3},{3,0},{4,5},{5,6},{6,7},{7,4},{8,9},{9,10},{10,1... | collective-permute-start | bytes 589832 | tf_op jit(solution)/shard_map/ppermute | solution.py:282
  40.8 13.4 %collective-permute-start.5 = (bf16[4,4,96,256]{3,2,1,0:T(8,128)(2,1)}, bf16[4,4,96,256]{3,2,1,0:T(8,128)(2,1)S(1)}, u32[]{:S(2)}, u32[]{:S(2)}) collective-permute-start(bf16[4,4,96,256]{3,2,1,0:T(8,128)(2,1)} %pad_maximum_fusion.2.refs_4_), channel_id=1, source_target_pairs={{0,32},{4,228},{32,64},{36,4},{64,96},{68,36},{96,128},{100,68},{1... | collective-permute-start | bytes 2359304 | tf_op jit(solution)/shard_map/ppermute | solution.py:319
  42.0 8.8 %collective-permute-start.20 = (bf16[8,96,256]{2,1,0:T(8,128)(2,1)S(1)}, bf16[8,96,256]{2,1,0:T(8,128)(2,1)S(1)}, u32[]{:S(2)}, u32[]{:S(2)}) collective-permute-start(bf16[8,96,256]{2,1,0:T(8,128)(2,1)S(1)} %get-tuple-element.16), channel_id=1, source_target_pairs={{0,8},{8,16},{16,24},{24,0},{1,9},{9,17},{17,25},{25,1},{2,10},{10... | collective-permute-start | bytes 1179656 | tf_op jit(solution)/shard_map/ppermute | solution.py:282
  44.0 10.2 %collective-permute-start.19 = (bf16[8,96,256]{2,1,0:T(8,128)(2,1)S(1)}, bf16[8,96,256]{2,1,0:T(8,128)(2,1)S(1)}, u32[]{:S(2)}, u32[]{:S(2)}) collective-permute-start(bf16[8,96,256]{2,1,0:T(8,128)(2,1)S(1)} %get-tuple-element.16), channel_id=1, source_target_pairs={{0,24},{8,0},{16,8},{24,16},{1,25},{9,1},{17,9},{25,17},{2,26},{10... | collective-permute-start | bytes 1179656 | tf_op jit(solution)/shard_map/ppermute | solution.py:282
  44.2 12.2 %collective-permute-start.31 = (bf16[8,96,256]{2,1,0:T(8,128)(2,1)S(1)}, bf16[8,96,256]{2,1,0:T(8,128)(2,1)S(1)}, u32[]{:S(2)}, u32[]{:S(2)}) collective-permute-start(bf16[8,96,256]{2,1,0:T(8,128)(2,1)S(1)} %get-tuple-element.15), channel_id=1, source_target_pairs={{0,1},{1,2},{2,3},{3,0},{4,5},{5,6},{6,7},{7,4},{8,9},{9,10},{10,1... | collective-permute-start | bytes 1179656 | tf_op jit(solution)/shard_map/ppermute | solution.py:282
  45.7 11.7 %collective-permute-start.30 = (bf16[8,96,256]{2,1,0:T(8,128)(2,1)S(1)}, bf16[8,96,256]{2,1,0:T(8,128)(2,1)S(1)}, u32[]{:S(2)}, u32[]{:S(2)}) collective-permute-start(bf16[8,96,256]{2,1,0:T(8,128)(2,1)S(1)} %get-tuple-element.15), channel_id=1, source_target_pairs={{0,3},{1,0},{2,1},{3,2},{4,7},{5,4},{6,5},{7,6},{8,11},{9,8},{10,9... | collective-permute-start | bytes 1179656 | tf_op jit(solution)/shard_map/ppermute | solution.py:282
  50.8 20.4 %collective-permute-start.4 = (bf16[4,4,96,256]{3,2,1,0:T(8,128)(2,1)}, bf16[4,4,96,256]{3,2,1,0:T(8,128)(2,1)S(1)}, u32[]{:S(2)}, u32[]{:S(2)}) collective-permute-start(bf16[4,4,96,256]{3,2,1,0:T(8,128)(2,1)} %pad_maximum_fusion.2.refs_4_), channel_id=1, source_target_pairs={{0,4},{4,0},{1,5},{5,1},{2,6},{6,2},{3,7},{7,3},{8,12},{12,8},{9,1... | collective-permute-start | bytes 2359304 | tf_op jit(solution)/shard_map/ppermute | solution.py:309
  54.3 19.0 %collective-permute-start.9 = (bf16[4,4,96,256]{3,2,1,0:T(8,128)(2,1)S(1)}, bf16[4,4,96,256]{3,2,1,0:T(8,128)(2,1)S(1)}, u32[]{:S(2)}, u32[]{:S(2)}) collective-permute-start(bf16[4,4,96,256]{3,2,1,0:T(8,128)(2,1)S(1)} %collective-permute-done.5.refs_6_), channel_id=1, source_target_pairs={{0,32},{4,228},{32,64},{36,4},{64,96},{68,36},{96,128},{100,68},{1... | collective-permute-start | bytes 2359304 | tf_op jit(solution)/shard_map/ppermute | solution.py:319
  54.3 5.7 %collective-permute-start.21 = (bf16[4,96,256]{2,1,0:T(8,128)(2,1)S(1)}, bf16[4,96,256]{2,1,0:T(8,128)(2,1)S(1)}, u32[]{:S(2)}, u32[]{:S(2)}) collective-permute-start(bf16[4,96,256]{2,1,0:T(8,128)(2,1)S(1)} %slice.37), channel_id=1, source_target_pairs={{0,8},{8,16},{16,24},{24,0},{1,9},{9,17},{17,25},{25,1},{2,10},{10... | collective-permute-start | bytes 589832 | tf_op jit(solution)/shard_map/ppermute | solution.py:282
  56.4 6.5 %collective-permute-start.22 = (bf16[4,96,256]{2,1,0:T(8,128)(2,1)S(1)}, bf16[4,96,256]{2,1,0:T(8,128)(2,1)S(1)}, u32[]{:S(2)}, u32[]{:S(2)}) collective-permute-start(bf16[4,96,256]{2,1,0:T(8,128)(2,1)S(1)} %slice.38), channel_id=1, source_target_pairs={{0,24},{8,0},{16,8},{24,16},{1,25},{9,1},{17,9},{25,17},{2,26},{10... | collective-permute-start | bytes 589832 | tf_op jit(solution)/shard_map/ppermute | solution.py:282
  57.4 13.6 %collective-permute-start = (bf16[96,512]{1,0:T(8,128)(2,1)S(1)}, bf16[96,512]{1,0:T(8,128)(2,1)S(1)}, u32[]{:S(2)}, u32[]{:S(2)}) collective-permute-start(bf16[96,512]{1,0:T(8,128)(2,1)S(1)} %slice.27), channel_id=1, source_target_pairs={{0,4},{4,8},{8,12},{12,16},{16,20},{20,24},{24,28},{28,32},{32,36}... | collective-permute-start | bytes 294920 | tf_op jit(solution)/shard_map/ppermute | solution.py:340
  60.0 8.3 %collective-permute-start.32 = (bf16[4,96,256]{2,1,0:T(8,128)(2,1)S(1)}, bf16[4,96,256]{2,1,0:T(8,128)(2,1)S(1)}, u32[]{:S(2)}, u32[]{:S(2)}) collective-permute-start(bf16[4,96,256]{2,1,0:T(8,128)(2,1)S(1)} %slice.40), channel_id=1, source_target_pairs={{0,1},{1,2},{2,3},{3,0},{4,5},{5,6},{6,7},{7,4},{8,9},{9,10},{10,1... | collective-permute-start | bytes 589832 | tf_op jit(solution)/shard_map/ppermute | solution.py:282
  62.9 6.8 %collective-permute-start.33 = (bf16[4,96,256]{2,1,0:T(8,128)(2,1)S(1)}, bf16[4,96,256]{2,1,0:T(8,128)(2,1)S(1)}, u32[]{:S(2)}, u32[]{:S(2)}) collective-permute-start(bf16[4,96,256]{2,1,0:T(8,128)(2,1)S(1)} %slice.41), channel_id=1, source_target_pairs={{0,3},{1,0},{2,1},{3,2},{4,7},{5,4},{6,5},{7,6},{8,11},{9,8},{10,9... | collective-permute-start | bytes 589832 | tf_op jit(solution)/shard_map/ppermute | solution.py:282
  68.3 21.6 %collective-permute-start.24 = (bf16[4,8,96,256]{3,2,1,0:T(8,128)(2,1)S(1)}, bf16[4,8,96,256]{3,2,1,0:T(8,128)(2,1)S(1)}, u32[]{:S(2)}, u32[]{:S(2)}) collective-permute-start(bf16[4,8,96,256]{3,2,1,0:T(8,128)(2,1)S(1)} %pad_maximum_fusion.refs_4_), channel_id=1, source_target_pairs={{0,1},{4,7},{1,2},{5,4},{2,3},{6,5},{3,0},{7,6},{8,9},{12,15},{9,1... | collective-permute-start | bytes 4718600 | tf_op jit(solution)/shard_map/ppermute | solution.py:319
  69.8 4.1 %collective-permute-start.7 = (bf16[4,4,96,256]{3,2,1,0:T(8,128)(2,1)S(1)}, bf16[4,4,96,256]{3,2,1,0:T(8,128)(2,1)S(1)}, u32[]{:S(2)}, u32[]{:S(2)}) collective-permute-start(bf16[4,4,96,256]{3,2,1,0:T(8,128)(2,1)S(1)} %collective-permute-done.5.refs_6_), channel_id=1, source_target_pairs={{0,4},{4,0},{1,5},{5,1},{2,6},{6,2},{3,7},{7,3},{8,12},{12,8},{9,1... | collective-permute-start | bytes 2359304 | tf_op jit(solution)/shard_map/ppermute | solution.py:309
  70.8 94.8 %copy-start.25 = (f32[3,256]{1,0:T(4,128)S(1)}, f32[3,256]{1,0:T(4,128)}, u32[]{:S(2)}) copy-start(f32[3,256]{1,0:T(4,128)} %param.13) | copy-start | bytes 9220
  70.8 94.8 %copy-start.26 = (f32[3,256]{1,0:T(4,128)S(1)}, f32[3,256]{1,0:T(4,128)}, u32[]{:S(2)}) copy-start(f32[3,256]{1,0:T(4,128)} %param.14) | copy-start | bytes 9220
  70.8 94.8 %copy-start.22 = (f32[3,31,256]{2,1,0:T(8,128)S(1)}, f32[3,31,256]{2,1,0:T(8,128)}, u32[]{:S(2)}) copy-start(f32[3,31,256]{2,1,0:T(8,128)} %param.12) | copy-start | bytes 285700
  71.0 127.2 %copy-start.1 = (bf16[4,8,96,256]{3,2,1,0:T(8,128)(2,1)}, bf16[4,8,96,256]{3,2,1,0:T(8,128)(2,1)S(1)}, u32[]{:S(2)}) copy-start(bf16[4,8,96,256]{3,2,1,0:T(8,128)(2,1)S(1)} %pad_maximum_fusion.1.refs_12_) | copy-start | bytes 4718596
  71.0 100.4 %copy-start.24 = (f32[3,2048]{1,0:T(4,128)S(1)}, f32[3,2048]{1,0:T(4,128)}, u32[]{:S(2)}) copy-start(f32[3,2048]{1,0:T(4,128)} %param.9) | copy-start | bytes 73732
  71.1 101.6 %copy-start.23 = (bf16[96,512]{1,0:T(8,128)(2,1)}, bf16[96,512]{1,0:T(8,128)(2,1)S(1)}, u32[]{:S(2)}) copy-start(bf16[96,512]{1,0:T(8,128)(2,1)S(1)} %collective-permute-done.before_ref) | copy-start | bytes 294916
  71.1 18.9 %collective-permute-start.23 = (bf16[4,8,96,256]{3,2,1,0:T(8,128)(2,1)S(1)}, bf16[4,8,96,256]{3,2,1,0:T(8,128)(2,1)S(1)}, u32[]{:S(2)}, u32[]{:S(2)}) collective-permute-start(bf16[4,8,96,256]{3,2,1,0:T(8,128)(2,1)S(1)} %pad_maximum_fusion.refs_4_), channel_id=1, source_target_pairs={{0,4},{4,0},{1,5},{5,1},{2,6},{6,2},{3,7},{7,3},{8,12},{12,8},{9,1... | collective-permute-start | bytes 4718600 | tf_op jit(solution)/shard_map/ppermute | solution.py:309
  71.2 92.8 %copy-start.8 = (bf16[4,4,96,256]{3,2,1,0:T(8,128)(2,1)}, bf16[4,4,96,256]{3,2,1,0:T(8,128)(2,1)S(1)}, u32[]{:S(2)}) copy-start(bf16[4,4,96,256]{3,2,1,0:T(8,128)(2,1)S(1)} %collective-permute-done.4.refs_5_) | copy-start | bytes 2359300
  71.2 20.6 %collective-permute-start.35 = (bf16[4,8,96,256]{3,2,1,0:T(8,128)(2,1)S(1)}, bf16[4,8,96,256]{3,2,1,0:T(8,128)(2,1)}, u32[]{:S(2)}, u32[]{:S(2)}) collective-permute-start(bf16[4,8,96,256]{3,2,1,0:T(8,128)(2,1)S(1)} %pad_maximum_fusion.1.refs_12_), channel_id=1, source_target_pairs={{0,8},{4,28},{8,16},{12,4},{16,24},{20,12},{24,0},{28,20},{1,9},{5... | collective-permute-start | bytes 4718600 | tf_op jit(solution)/shard_map/ppermute | solution.py:319
  73.3 90.7 %copy-start.9 = (bf16[4,4,96,256]{3,2,1,0:T(8,128)(2,1)}, bf16[4,4,96,256]{3,2,1,0:T(8,128)(2,1)S(1)}, u32[]{:S(2)}) copy-start(bf16[4,4,96,256]{3,2,1,0:T(8,128)(2,1)S(1)} %collective-permute-done.9.refs_10_) | copy-start | bytes 2359300
  73.3 14.6 %collective-permute-start.6 = (bf16[4,4,96,256]{3,2,1,0:T(8,128)(2,1)S(1)}, bf16[4,4,96,256]{3,2,1,0:T(8,128)(2,1)S(1)}, u32[]{:S(2)}, u32[]{:S(2)}) collective-permute-start(bf16[4,4,96,256]{3,2,1,0:T(8,128)(2,1)S(1)} %collective-permute-done.4.refs_5_), channel_id=1, source_target_pairs={{0,32},{4,228},{32,64},{36,4},{64,96},{68,36},{96,128},{100,68},{1... | collective-permute-start | bytes 2359304 | tf_op jit(solution)/shard_map/ppermute | solution.py:319
  73.9 90.7 %copy-start.10 = (bf16[4,4,96,256]{3,2,1,0:T(8,128)(2,1)}, bf16[4,4,96,256]{3,2,1,0:T(8,128)(2,1)S(1)}, u32[]{:S(2)}) copy-start(bf16[4,4,96,256]{3,2,1,0:T(8,128)(2,1)S(1)} %collective-permute-done.7.refs_8_) | copy-start | bytes 2359300
  73.9 27.2 %collective-permute-start.34 = (bf16[4,8,96,256]{3,2,1,0:T(8,128)(2,1)S(1)}, bf16[4,8,96,256]{3,2,1,0:T(8,128)(2,1)S(1)}, u32[]{:S(2)}, u32[]{:S(2)}) collective-permute-start(bf16[4,8,96,256]{3,2,1,0:T(8,128)(2,1)S(1)} %pad_maximum_fusion.1.refs_12_), channel_id=1, source_target_pairs={{0,4},{4,0},{1,5},{5,1},{2,6},{6,2},{3,7},{7,3},{8,12},{12,8},{9,1... | collective-permute-start | bytes 4718600 | tf_op jit(solution)/shard_map/ppermute | solution.py:309
  87.9 76.7 %copy-start.11 = (bf16[4,4,96,256]{3,2,1,0:T(8,128)(2,1)}, bf16[4,4,96,256]{3,2,1,0:T(8,128)(2,1)S(1)}, u32[]{:S(2)}) copy-start(bf16[4,4,96,256]{3,2,1,0:T(8,128)(2,1)S(1)} %collective-permute-done.6.refs_7_) | copy-start | bytes 2359300
  87.9 13.2 %collective-permute-start.13 = (bf16[4,4,96,256]{3,2,1,0:T(8,128)(2,1)S(1)}, bf16[4,4,96,256]{3,2,1,0:T(8,128)(2,1)S(1)}, u32[]{:S(2)}, u32[]{:S(2)}) collective-permute-start(bf16[4,4,96,256]{3,2,1,0:T(8,128)(2,1)S(1)} %collective-permute-done.9.refs_10_), channel_id=1, source_target_pairs={{0,32},{4,228},{32,64},{36,4},{64,96},{68,36},{96,128},{100,68},{1... | collective-permute-start | bytes 2359304 | tf_op jit(solution)/shard_map/ppermute | solution.py:319
  90.0 28.0 %copy-start.3 = (bf16[4,8,96,256]{3,2,1,0:T(8,128)(2,1)}, bf16[4,8,96,256]{3,2,1,0:T(8,128)(2,1)S(1)}, u32[]{:S(2)}) copy-start(bf16[4,8,96,256]{3,2,1,0:T(8,128)(2,1)S(1)} %collective-permute-done.24.refs_6_) | copy-start | bytes 4718596
  90.0 19.6 %collective-permute-start.10 = (bf16[4,4,96,256]{3,2,1,0:T(8,128)(2,1)S(1)}, bf16[4,4,96,256]{3,2,1,0:T(8,128)(2,1)S(1)}, u32[]{:S(2)}, u32[]{:S(2)}) collective-permute-start(bf16[4,4,96,256]{3,2,1,0:T(8,128)(2,1)S(1)} %collective-permute-done.6.refs_7_), channel_id=1, source_target_pairs={{0,32},{4,228},{32,64},{36,4},{64,96},{68,36},{96,128},{100,68},{1... | collective-permute-start | bytes 2359304 | tf_op jit(solution)/shard_map/ppermute | solution.py:319
  90.0 42.0 %copy-start.4 = (bf16[4,8,96,256]{3,2,1,0:T(8,128)(2,1)}, bf16[4,8,96,256]{3,2,1,0:T(8,128)(2,1)S(1)}, u32[]{:S(2)}) copy-start(bf16[4,8,96,256]{3,2,1,0:T(8,128)(2,1)S(1)} %collective-permute-done.23.refs_5_) | copy-start | bytes 4718596
  90.0 19.6 %collective-permute-start.11 = (bf16[4,4,96,256]{3,2,1,0:T(8,128)(2,1)S(1)}, bf16[4,4,96,256]{3,2,1,0:T(8,128)(2,1)S(1)}, u32[]{:S(2)}, u32[]{:S(2)}) collective-permute-start(bf16[4,4,96,256]{3,2,1,0:T(8,128)(2,1)S(1)} %collective-permute-done.9.refs_10_), channel_id=1, source_target_pairs={{0,4},{4,0},{1,5},{5,1},{2,6},{6,2},{3,7},{7,3},{8,12},{12,8},{9,1... | collective-permute-start | bytes 2359304 | tf_op jit(solution)/shard_map/ppermute | solution.py:309
  91.8 17.9 %collective-permute-start.8 = (bf16[4,4,96,256]{3,2,1,0:T(8,128)(2,1)S(1)}, bf16[4,4,96,256]{3,2,1,0:T(8,128)(2,1)S(1)}, u32[]{:S(2)}, u32[]{:S(2)}) collective-permute-start(bf16[4,4,96,256]{3,2,1,0:T(8,128)(2,1)S(1)} %collective-permute-done.6.refs_7_), channel_id=1, source_target_pairs={{0,4},{4,0},{1,5},{5,1},{2,6},{6,2},{3,7},{7,3},{8,12},{12,8},{9,1... | collective-permute-start | bytes 2359304 | tf_op jit(solution)/shard_map/ppermute | solution.py:309
  101.1 97.1 %copy-start.12 = (bf16[4,4,96,256]{3,2,1,0:T(8,128)(2,1)}, bf16[4,4,96,256]{3,2,1,0:T(8,128)(2,1)S(1)}, u32[]{:S(2)}) copy-start(bf16[4,4,96,256]{3,2,1,0:T(8,128)(2,1)S(1)} %collective-permute-done.13.refs_14_) | copy-start | bytes 2359300
  101.1 16.9 %collective-permute-start.17 = (bf16[4,4,96,256]{3,2,1,0:T(8,128)(2,1)S(1)}, bf16[4,4,96,256]{3,2,1,0:T(8,128)(2,1)S(1)}, u32[]{:S(2)}, u32[]{:S(2)}) collective-permute-start(bf16[4,4,96,256]{3,2,1,0:T(8,128)(2,1)S(1)} %collective-permute-done.13.refs_14_), channel_id=1, source_target_pairs={{0,32},{4,228},{32,64},{36,4},{64,96},{68,36},{96,128},{100,68},{1... | collective-permute-start | bytes 2359304 | tf_op jit(solution)/shard_map/ppermute | solution.py:319
  101.1 47.7 %copy-start.5 = (bf16[4,8,96,256]{3,2,1,0:T(8,128)(2,1)}, bf16[4,8,96,256]{3,2,1,0:T(8,128)(2,1)S(1)}, u32[]{:S(2)}) copy-start(bf16[4,8,96,256]{3,2,1,0:T(8,128)(2,1)S(1)} %collective-permute-done.34.refs_13_) | copy-start | bytes 4718596
  101.1 16.8 %collective-permute-start.15 = (bf16[4,4,96,256]{3,2,1,0:T(8,128)(2,1)S(1)}, bf16[4,4,96,256]{3,2,1,0:T(8,128)(2,1)S(1)}, u32[]{:S(2)}, u32[]{:S(2)}) collective-permute-start(bf16[4,4,96,256]{3,2,1,0:T(8,128)(2,1)S(1)} %collective-permute-done.13.refs_14_), channel_id=1, source_target_pairs={{0,4},{4,0},{1,5},{5,1},{2,6},{6,2},{3,7},{7,3},{8,12},{12,8},{9,1... | collective-permute-start | bytes 2359304 | tf_op jit(solution)/shard_map/ppermute | solution.py:309
  109.5 55.2 %copy-start.13 = (bf16[4,4,96,256]{3,2,1,0:T(8,128)(2,1)}, bf16[4,4,96,256]{3,2,1,0:T(8,128)(2,1)S(1)}, u32[]{:S(2)}) copy-start(bf16[4,4,96,256]{3,2,1,0:T(8,128)(2,1)S(1)} %collective-permute-done.10.refs_11_) | copy-start | bytes 2359300
  109.5 16.9 %collective-permute-start.14 = (bf16[4,4,96,256]{3,2,1,0:T(8,128)(2,1)S(1)}, bf16[4,4,96,256]{3,2,1,0:T(8,128)(2,1)S(1)}, u32[]{:S(2)}, u32[]{:S(2)}) collective-permute-start(bf16[4,4,96,256]{3,2,1,0:T(8,128)(2,1)S(1)} %collective-permute-done.10.refs_11_), channel_id=1, source_target_pairs={{0,32},{4,228},{32,64},{36,4},{64,96},{68,36},{96,128},{100,68},{1... | collective-permute-start | bytes 2359304 | tf_op jit(solution)/shard_map/ppermute | solution.py:319
  109.6 16.9 %collective-permute-start.12 = (bf16[4,4,96,256]{3,2,1,0:T(8,128)(2,1)S(1)}, bf16[4,4,96,256]{3,2,1,0:T(8,128)(2,1)S(1)}, u32[]{:S(2)}, u32[]{:S(2)}) collective-permute-start(bf16[4,4,96,256]{3,2,1,0:T(8,128)(2,1)S(1)} %collective-permute-done.10.refs_11_), channel_id=1, source_target_pairs={{0,4},{4,0},{1,5},{5,1},{2,6},{6,2},{3,7},{7,3},{8,12},{12,8},{9,1... | collective-permute-start | bytes 2359304 | tf_op jit(solution)/shard_map/ppermute | solution.py:309
  109.7 22.3 %collective-permute-start.28 = (bf16[4,8,96,256]{3,2,1,0:T(8,128)(2,1)S(1)}, bf16[4,8,96,256]{3,2,1,0:T(8,128)(2,1)}, u32[]{:S(2)}, u32[]{:S(2)}) collective-permute-start(bf16[4,8,96,256]{3,2,1,0:T(8,128)(2,1)S(1)} %collective-permute-done.24.refs_6_), channel_id=1, source_target_pairs={{0,1},{4,7},{1,2},{5,4},{2,3},{6,5},{3,0},{7,6},{8,9},{12,15},{9,1... | collective-permute-start | bytes 4718600 | tf_op jit(solution)/shard_map/ppermute | solution.py:319
  118.0 46.8 %copy-start.16 = (bf16[4,4,96,256]{3,2,1,0:T(8,128)(2,1)}, bf16[4,4,96,256]{3,2,1,0:T(8,128)(2,1)S(1)}, u32[]{:S(2)}) copy-start(bf16[4,4,96,256]{3,2,1,0:T(8,128)(2,1)S(1)} %collective-permute-done.17.refs_18_) | copy-start | bytes 2359300
  118.0 14.0 %collective-permute-start.26 = (bf16[4,8,96,256]{3,2,1,0:T(8,128)(2,1)S(1)}, bf16[4,8,96,256]{3,2,1,0:T(8,128)(2,1)S(1)}, u32[]{:S(2)}, u32[]{:S(2)}) collective-permute-start(bf16[4,8,96,256]{3,2,1,0:T(8,128)(2,1)S(1)} %collective-permute-done.24.refs_6_), channel_id=1, source_target_pairs={{0,4},{4,0},{1,5},{5,1},{2,6},{6,2},{3,7},{7,3},{8,12},{12,8},{9,1... | collective-permute-start | bytes 4718600 | tf_op jit(solution)/shard_map/ppermute | solution.py:309
  118.0 46.8 %copy-start.17 = (bf16[4,4,96,256]{3,2,1,0:T(8,128)(2,1)}, bf16[4,4,96,256]{3,2,1,0:T(8,128)(2,1)S(1)}, u32[]{:S(2)}) copy-start(bf16[4,4,96,256]{3,2,1,0:T(8,128)(2,1)S(1)} %collective-permute-done.15.refs_16_) | copy-start | bytes 2359300
  118.0 30.8 %collective-permute-start.25 = (bf16[4,8,96,256]{3,2,1,0:T(8,128)(2,1)S(1)}, bf16[4,8,96,256]{3,2,1,0:T(8,128)(2,1)}, u32[]{:S(2)}, u32[]{:S(2)}) collective-permute-start(bf16[4,8,96,256]{3,2,1,0:T(8,128)(2,1)S(1)} %collective-permute-done.23.refs_5_), channel_id=1, source_target_pairs={{0,1},{4,7},{1,2},{5,4},{2,3},{6,5},{3,0},{7,6},{8,9},{12,15},{9,1... | collective-permute-start | bytes 4718600 | tf_op jit(solution)/shard_map/ppermute | solution.py:319
  126.4 38.4 %copy-start.18 = (bf16[4,4,96,256]{3,2,1,0:T(8,128)(2,1)}, bf16[4,4,96,256]{3,2,1,0:T(8,128)(2,1)S(1)}, u32[]{:S(2)}) copy-start(bf16[4,4,96,256]{3,2,1,0:T(8,128)(2,1)S(1)} %collective-permute-done.14.refs_15_) | copy-start | bytes 2359300
  126.4 22.4 %collective-permute-start.39 = (bf16[4,8,96,256]{3,2,1,0:T(8,128)(2,1)}, bf16[4,8,96,256]{3,2,1,0:T(8,128)(2,1)}, u32[]{:S(2)}, u32[]{:S(2)}) collective-permute-start(bf16[4,8,96,256]{3,2,1,0:T(8,128)(2,1)} %collective-permute-done.35.refs_14_), channel_id=1, source_target_pairs={{0,8},{4,28},{8,16},{12,4},{16,24},{20,12},{24,0},{28,20},{1,9},{5... | collective-permute-start | bytes 4718600 | tf_op jit(solution)/shard_map/ppermute | solution.py:319
  126.5 38.3 %copy-start.19 = (bf16[4,4,96,256]{3,2,1,0:T(8,128)(2,1)}, bf16[4,4,96,256]{3,2,1,0:T(8,128)(2,1)S(1)}, u32[]{:S(2)}) copy-start(bf16[4,4,96,256]{3,2,1,0:T(8,128)(2,1)S(1)} %collective-permute-done.12.refs_13_) | copy-start | bytes 2359300
  126.5 37.5 %collective-permute-start.36 = (bf16[4,8,96,256]{3,2,1,0:T(8,128)(2,1)S(1)}, bf16[4,8,96,256]{3,2,1,0:T(8,128)(2,1)}, u32[]{:S(2)}, u32[]{:S(2)}) collective-permute-start(bf16[4,8,96,256]{3,2,1,0:T(8,128)(2,1)S(1)} %collective-permute-done.34.refs_13_), channel_id=1, source_target_pairs={{0,8},{4,28},{8,16},{12,4},{16,24},{20,12},{24,0},{28,20},{1,9},{5... | collective-permute-start | bytes 4718600 | tf_op jit(solution)/shard_map/ppermute | solution.py:319
  132.0 32.0 %collective-permute-start.18 = (bf16[4,4,96,256]{3,2,1,0:T(8,128)(2,1)S(1)}, bf16[4,4,96,256]{3,2,1,0:T(8,128)(2,1)S(1)}, u32[]{:S(2)}, u32[]{:S(2)}) collective-permute-start(bf16[4,4,96,256]{3,2,1,0:T(8,128)(2,1)S(1)} %collective-permute-done.17.refs_18_), channel_id=1, source_target_pairs={{0,4},{4,0},{1,5},{5,1},{2,6},{6,2},{3,7},{7,3},{8,12},{12,8},{9,1... | collective-permute-start | bytes 2359304 | tf_op jit(solution)/shard_map/ppermute | solution.py:309
  132.0 32.0 %copy-start.6 = (bf16[4,8,96,256]{3,2,1,0:T(8,128)(2,1)}, bf16[4,8,96,256]{3,2,1,0:T(8,128)(2,1)S(1)}, u32[]{:S(2)}) copy-start(bf16[4,8,96,256]{3,2,1,0:T(8,128)(2,1)S(1)} %collective-permute-done.26.refs_8_) | copy-start | bytes 4718596
  132.0 32.6 %collective-permute-start.16 = (bf16[4,4,96,256]{3,2,1,0:T(8,128)(2,1)S(1)}, bf16[4,4,96,256]{3,2,1,0:T(8,128)(2,1)S(1)}, u32[]{:S(2)}, u32[]{:S(2)}) collective-permute-start(bf16[4,4,96,256]{3,2,1,0:T(8,128)(2,1)S(1)} %collective-permute-done.14.refs_15_), channel_id=1, source_target_pairs={{0,4},{4,0},{1,5},{5,1},{2,6},{6,2},{3,7},{7,3},{8,12},{12,8},{9,1... | collective-permute-start | bytes 2359304 | tf_op jit(solution)/shard_map/ppermute | solution.py:309
  148.8 64.8 %collective-permute-start.37 = (bf16[4,8,96,256]{3,2,1,0:T(8,128)(2,1)}, bf16[4,8,96,256]{3,2,1,0:T(8,128)(2,1)}, u32[]{:S(2)}, u32[]{:S(2)}) collective-permute-start(bf16[4,8,96,256]{3,2,1,0:T(8,128)(2,1)} %collective-permute-done.35.refs_14_), channel_id=1, source_target_pairs={{0,4},{4,0},{1,5},{5,1},{2,6},{6,2},{3,7},{7,3},{8,12},{12,8},{9,1... | collective-permute-start | bytes 4718600 | tf_op jit(solution)/shard_map/ppermute | solution.py:309
  148.8 64.8 %collective-permute-start.29 = (bf16[4,8,96,256]{3,2,1,0:T(8,128)(2,1)}, bf16[4,8,96,256]{3,2,1,0:T(8,128)(2,1)}, u32[]{:S(2)}, u32[]{:S(2)}) collective-permute-start(bf16[4,8,96,256]{3,2,1,0:T(8,128)(2,1)} %collective-permute-done.28.refs_10_), channel_id=1, source_target_pairs={{0,4},{4,0},{1,5},{5,1},{2,6},{6,2},{3,7},{7,3},{8,12},{12,8},{9,1... | collective-permute-start | bytes 4718600 | tf_op jit(solution)/shard_map/ppermute | solution.py:309
  164.0 49.6 %collective-permute-start.27 = (bf16[4,8,96,256]{3,2,1,0:T(8,128)(2,1)}, bf16[4,8,96,256]{3,2,1,0:T(8,128)(2,1)}, u32[]{:S(2)}, u32[]{:S(2)}) collective-permute-start(bf16[4,8,96,256]{3,2,1,0:T(8,128)(2,1)} %collective-permute-done.25.refs_7_), channel_id=1, source_target_pairs={{0,4},{4,0},{1,5},{5,1},{2,6},{6,2},{3,7},{7,3},{8,12},{12,8},{9,1... | collective-permute-start | bytes 4718600 | tf_op jit(solution)/shard_map/ppermute | solution.py:309
  164.0 49.6 %collective-permute-start.40 = (bf16[4,8,96,256]{3,2,1,0:T(8,128)(2,1)}, bf16[4,8,96,256]{3,2,1,0:T(8,128)(2,1)}, u32[]{:S(2)}, u32[]{:S(2)}) collective-permute-start(bf16[4,8,96,256]{3,2,1,0:T(8,128)(2,1)} %collective-permute-done.39.refs_18_), channel_id=1, source_target_pairs={{0,4},{4,0},{1,5},{5,1},{2,6},{6,2},{3,7},{7,3},{8,12},{12,8},{9,1... | collective-permute-start | bytes 4718600 | tf_op jit(solution)/shard_map/ppermute | solution.py:309
  164.6 49.0 %collective-permute-start.38 = (bf16[4,8,96,256]{3,2,1,0:T(8,128)(2,1)}, bf16[4,8,96,256]{3,2,1,0:T(8,128)(2,1)}, u32[]{:S(2)}, u32[]{:S(2)}) collective-permute-start(bf16[4,8,96,256]{3,2,1,0:T(8,128)(2,1)} %collective-permute-done.36.refs_15_), channel_id=1, source_target_pairs={{0,4},{4,0},{1,5},{5,1},{2,6},{6,2},{3,7},{7,3},{8,12},{12,8},{9,1... | collective-permute-start | bytes 4718600 | tf_op jit(solution)/shard_map/ppermute | solution.py:309
  166.4 14.4 %all-to-all-start.1 = ((f32[4,3,33,256]{3,2,1,0:T(8,128)}), f32[4,3,33,256]{3,2,1,0:T(8,128)S(1)}, u32[]{:S(2)}, u32[]{:S(2)}) async-start(f32[4,3,33,256]{3,2,1,0:T(8,128)} %broadcast_in_dim.17), calls=%async_computation.1 | async-start | bytes 983040 | tf_op jit(solution)/shard_map/all_to_all | solution.py:286
  (7 other events, 42.1 us)
